TPU v7x, 32 devices: a whole 2x2x4 slice. The times are simulated.
32 devices in a mesh: sp: 8 (over z, y), tp: 4 (over x, core).
Axes of the slice: x: 2, y: 2, z: 4, core: 2. Of those that a mesh axis runs over, the one named last changes fastest.
Arguments:
- target: bfloat16 [1024, 2048], P('sp'), may hold values from -160 to 160
- source: bfloat16 [2048, 2048], P(('sp', 'tp')), may hold values from -160 to 160
- query_gain: float32 [2048], replicated, may hold values from 0.1 to 1.9
- source_gain: float32 [2048], replicated, may hold values from 0.1 to 1.9
- query_weight: bfloat16 [2048, 2048], P(None, 'tp'), may hold values from -4 to 4
- key_weight: bfloat16 [2048, 512], replicated, may hold values from -4 to 4
- value_weight: bfloat16 [2048, 512], replicated, may hold values from -1 to 1
- out_weight: bfloat16 [2048, 2048], P('tp'), may hold values from -0.125 to 0.125
- mixer_gain: float32 [2048], replicated, may hold values from 0.1 to 1.9
- gate_weight: bfloat16 [2048, 3072], P(None, 'tp'), may hold values from -0.125 to 0.125
- up_weight: bfloat16 [2048, 3072], P(None, 'tp'), may hold values from -0.125 to 0.125
- gate_taps: bfloat16 [3, 3072], P(None, 'tp'), may hold values from -3.5 to 3.5
- up_taps: bfloat16 [3, 3072], P(None, 'tp'), may hold values from -3.5 to 3.5
- down_weight: bfloat16 [3072, 2048], P('tp'), may hold values from -0.109375 to 0.109375
- final_gain: float32 [2048], replicated, may hold values from 0.1 to 1.9
Outputs:
- layer_out: bfloat16 [1024, 2048], P(('sp', 'tp'))
All inputs are finite; a program needn't handle non-finite values.
Results may differ from a plain program's by a relative error of at most 0.012.
Values may be sent and summed in bfloat16 or wider, within the bound.
A program may use at most 64 MiB of HBM per device.

v0:
```python
import functools

import jax
import jax.numpy as jnp
from jax import lax
from jax.experimental import pallas as pl
from jax.experimental.pallas import tpu as pltpu
from jax.sharding import PartitionSpec as P

MESH = pl.DeviceIdType.MESH
EPS = 1e-06
HALO = 16
RUN = 32
CORES = 2
F32 = jnp.float32
BF16 = jnp.bfloat16


def normed(values, gain):
    wide = values.astype(F32)
    scale = lax.rsqrt(jnp.mean(wide * wide, axis=-1, keepdims=True) + EPS)
    return (wide * scale * gain).astype(BF16)


def layer(
    dims,
    target_h,
    source_h,
    qgain_h,
    sgain_h,
    qw_h,
    kw_h,
    vw_h,
    ow_h,
    mgain_h,
    gw_h,
    uw_h,
    gtaps_h,
    utaps_h,
    dw_h,
    fgain_h,
    out_ref,
    tgt,
    src,
    qgain,
    sgain,
    qw,
    kw,
    vw,
    ow,
    mgain,
    gw,
    uw,
    gtaps,
    utaps,
    dw,
    fgain,
    kvh,
    kv,
    q2,
    top,
    tot,
    acc,
    att,
    part,
    half_s,
    half_r,
    chip_s,
    chip_r,
    res,
    rows_in,
    conv_g,
    conv_u,
    hid,
    tail_s,
    tail_r,
    end_s,
    end_r,
    load_sem,
    kx_s,
    kx_r,
    cw_s,
    cw_r,
    cc_s,
    cc_r,
    d2_s,
    d2_r,
    b_s,
    b_r,
    bx_s,
    bx_r,
    m_s,
    m_r,
    h_s,
    h_r,
    f_s,
    f_r,
    fx_s,
    fx_r,
):
    n, chips, kv_heads, head, heads_here, cols, sub = dims
    tgt_rows, width = tgt.shape
    r = src.shape[0]
    rs = tgt_rows // (CORES * chips)
    half_rows = chips * rs
    run = r // sub
    runs = chips * sub
    chunks = width // cols
    sp = lax.axis_index("sp")
    tp = lax.axis_index("tp")
    chip = tp // CORES
    core = tp % CORES
    mate = tp + 1 - 2 * core

    def chip_at(k):
        return (chip + k) % chips

    def ring_at(p):
        if n % 2:
            return p
        upper = p // (n // 2)
        return 2 * (p * (1 - upper) + (n - 1 - p) * upper) + upper

    if n % 2:
        pos = sp
    else:
        pos = (sp // 2) * (1 - sp % 2) + (n - 1 - sp // 2) * (sp % 2)
    ahead = ring_at((pos + 1) % n)
    behind = ring_at((pos + n - 1) % n)

    def load(index, hbm, vmem):
        copy = pltpu.make_async_copy(hbm, vmem, load_sem.at[index])
        copy.start()
        return copy

    def head_of(c):
        return (c * CORES * kv_heads) // (chips * CORES)

    own_head = head_of(chip)
    order = [(own_head + 1 + g) % kv_heads for g in range(kv_heads)]

    def columns(g):
        return pl.ds(pl.multiple_of(g * head, head), head)

    first = [load(0, source_h, src), load(1, sgain_h, sgain)]
    by_head = [
        [
            load(2 + 2 * i, kw_h.at[:, columns(g)], kw.at[:, columns(g)]),
            load(3 + 2 * i, vw_h.at[:, columns(g)], vw.at[:, columns(g)]),
        ]
        for i, g in enumerate(order)
    ]
    used = 2 + 2 * kv_heads

    barrier = pltpu.get_barrier_semaphore()
    following = (sp + 1) % n
    peers = [(ahead, tp), (behind, tp), (sp, mate)]
    peers += [(sp, chip_at(k) * CORES + core) for k in range(1, chips)]
    for peer in peers:
        pl.semaphore_signal(barrier, inc=1, device_id=peer, device_id_type=MESH)

    def remote(source_ref, dest_ref, send, recv, device):
        return pltpu.make_async_remote_copy(
            src_ref=source_ref,
            dst_ref=dest_ref,
            send_sem=send,
            recv_sem=recv,
            device_id=device,
            device_id_type=MESH,
        )

    def block(slot, lineage, j):
        start = ((slot * CORES + lineage) * runs + j) * run
        if not isinstance(start, int):
            start = pl.multiple_of(start, run)
        return kv.at[pl.ds(start, run), :]

    def chip_copy(j):
        there = chip_at(j // sub)
        return remote(
            kvh.at[head_of(there), (j % sub) * run : (j % sub + 1) * run, :],
            block(0, 0, j),
            kx_s.at[j],
            kx_r.at[j],
            (sp, there * CORES + core),
        )

    last = n // 2 if n % 2 == 0 else 0
    full = (n - 1) // 2
    if sub > 1:
        half_cw = [j for j in range(runs) if j % sub < sub // 2]
    else:
        half_cw = list(range((runs + 1) // 2))
    half_cc = [j for j in range(runs) if j not in half_cw]

    def cw_slot(d):
        return 2 * d - 1

    def cc_slot(d):
        return n - 1 if isinstance(d, int) and d == last else 2 * d

    def cw_copy(d, j):
        held = 0 if isinstance(d, int) and d == 1 else cw_slot(d - 1)
        return remote(
            block(held, 0, j), block(cw_slot(d), 0, j), cw_s.at[d, j], cw_r.at[d, j], (ahead, tp)
        )

    def cc_copy(d, j):
        held = 0 if isinstance(d, int) and d == 1 else 2 * (d - 1)
        return remote(
            block(held, 0, j), block(cc_slot(d), 0, j), cc_s.at[d, j], cc_r.at[d, j], (behind, tp)
        )

    def mate_copy(slot, j):
        return remote(
            block(slot, 0, j), block(slot, 1, j), d2_s.at[slot, j], d2_r.at[slot, j], (sp, mate)
        )

    def launch(j):
        if n > 2 or j in half_cw:
            cw_copy(1, j).start()
        if n > 2 or j in half_cc:
            cc_copy(1, j).start()
        mate_copy(0, j).start()

    for copy in first:
        copy.wait()
    source_in = normed(src[...], sgain[...])
    second = [
        load(used + i, a, b)
        for i, (a, b) in enumerate(((target_h, tgt), (qgain_h, qgain), (qw_h, qw)))
    ]
    early = chips == kv_heads
    for i, g in enumerate(order):
        for copy in by_head[i]:
            copy.wait()
        keys = jnp.dot(source_in, kw[:, columns(g)], preferred_element_type=F32)
        kvh[g, :, :head] = keys.astype(BF16)
        values = jnp.dot(source_in, vw[:, columns(g)], preferred_element_type=F32)
        kvh[g, :, head:] = values.astype(BF16)
        if i == (kv_heads - 2 if early else kv_heads - 1):
            pl.semaphore_wait(barrier, len(peers))
            for j in range(sub, runs):
                chip_copy(j).start()
    kv[0:r, :] = kvh[own_head]
    for j in range(sub):
        launch(j)
    rest = [
        load(used + 3 + i, a, b)
        for i, (a, b) in enumerate(
            (
                (ow_h, ow),
                (mgain_h, mgain),
                (gw_h, gw),
                (uw_h, uw),
                (gtaps_h, gtaps),
                (utaps_h, utaps),
                (dw_h, dw),
                (fgain_h, fgain),
            )
        )
    ]

    for copy in second:
        copy.wait()
    queries = jnp.dot(normed(tgt[...], qgain[...]), qw[...], preferred_element_type=F32).astype(
        BF16
    )
    for h in range(heads_here):
        q2[h * tgt_rows : (h + 1) * tgt_rows, :] = queries[:, h * head : (h + 1) * head]
    top[...] = jnp.full(top.shape, -1e30, F32)
    tot[...] = jnp.zeros(tot.shape, F32)
    acc[...] = jnp.zeros(acc.shape, F32)

    for j in range(sub, runs):
        chip_copy(j).wait_recv()
        launch(j)

    slot_rows = CORES * chips * r

    def attend(slot, slots):
        start = slot * slot_rows
        if not isinstance(start, int):
            start = pl.multiple_of(start, slot_rows)
        for s in range(slots):
            for j in range(runs):
                mate_copy(slot + s, j).wait_recv()
        here = pl.ds(start, slots * slot_rows)
        scores = lax.dot_general(
            q2[...], kv[here, :head], (((1,), (1,)), ((), ())), preferred_element_type=F32
        ) * (head**-0.5)
        old = top[...]
        new = jnp.maximum(old, jnp.max(scores, axis=-1, keepdims=True))
        shrink = jnp.exp(old - new)
        probs = jnp.exp(scores - new)
        top[...] = new
        tot[...] = tot[...] * shrink + jnp.sum(probs, axis=-1, keepdims=True)
        acc[...] = acc[...] * shrink + jnp.dot(
            probs.astype(BF16), kv[here, head:], preferred_element_type=F32
        )

    def step(d, cw_on, cc_on):
        for j in range(runs):
            cw_copy(d, j).wait_recv()
            if j in cw_on:
                cw_copy(d + 1, j).start()
            mate_copy(cw_slot(d), j).start()
            cc_copy(d, j).wait_recv()
            if j in cc_on:
                cc_copy(d + 1, j).start()
            mate_copy(cc_slot(d), j).start()

    every = range(runs)
    few = half_cw if last else []
    others = half_cc if last else []
    if full >= 1:
        step(1, every if full > 1 else few, every if full > 1 else others)
        attend(0, 1)
        if full > 6:

            def middle(d, carry):
                step(d, every, every)
                attend(2 * d - 3, 2)
                return carry

            lax.fori_loop(2, full, middle, 0)
        else:
            for d in range(2, full):
                step(d, every, every)
                attend(2 * d - 3, 2)
        if full > 1:
            step(full, few, others)
            attend(2 * full - 3, 2)
        tail_slot, tail_count = 2 * full - 1, 2
    else:
        tail_slot, tail_count = 0, 1
    if last:
        for j in every:
            (cw_copy if j in half_cw else cc_copy)(last, j).wait_recv()
            mate_copy(n - 1, j).start()
    attend(tail_slot, tail_count)
    if last:
        attend(n - 1, 1)

    attended = (acc[...] / tot[...]).astype(BF16)
    for h in range(heads_here):
        att[:, h * head : (h + 1) * head] = attended[h * tgt_rows : (h + 1) * tgt_rows, :]
    for copy in rest:
        copy.wait()

    def piece(c, side):
        return pl.ds(pl.multiple_of((c * CORES + side) * rs, rs), rs)

    def multiply_out(lhs, weight, send, recv, send_sem, recv_sem):
        for c in range(chunks):
            here = slice(c * cols, (c + 1) * cols)
            part[c] = jnp.dot(lhs, weight[:, here], preferred_element_type=F32)
            for k in range(chips):
                send[c, k * rs : (k + 1) * rs, :] = part[c, piece(k, 1 - core), :].astype(BF16)
            remote(send.at[c], recv.at[c], send_sem.at[c], recv_sem.at[c], (sp, mate)).start()

    def mate_wait(c, send, recv, send_sem, recv_sem):
        remote(send.at[c], recv.at[c], send_sem.at[c], recv_sem.at[c], (sp, mate)).wait_recv()

    multiply_out(att[...], ow, half_s, half_r, b_s, b_r)

    def wide_copy(k, c):
        return remote(
            chip_s.at[c],
            chip_r.at[k - 1, c],
            bx_s.at[k, c],
            bx_r.at[k, c],
            (sp, chip_at(k) * CORES + core),
        )

    for c in range(chunks):
        mate_wait(c, half_s, half_r, b_s, b_r)
        for k in range(chips):
            at = slice(k * rs, (k + 1) * rs)
            both = part[c, piece(k, core), :] + half_r[c, at, :].astype(F32)
            res[at, c * cols : (c + 1) * cols] = both
            chip_s[c, at, :] = both.astype(BF16)
        for k in range(1, chips):
            wide_copy(k, c).start()
    squares = jnp.zeros((half_rows, 1), F32)
    for c in range(chunks):
        here = slice(c * cols, (c + 1) * cols)
        projected = res[:, here]
        for k in range(1, chips):
            wide_copy(k, c).wait_recv()
            projected = projected + chip_r[k - 1, c].astype(F32)
        mine = jnp.concatenate([tgt[piece(k, core), here] for k in range(chips)], axis=0)
        residual = (mine.astype(F32) + projected).astype(BF16).astype(F32)
        res[:, here] = residual
        squares = squares + jnp.sum(residual * residual, axis=-1, keepdims=True)
    scale = lax.rsqrt(squares / width + EPS)

    def spot(k):
        return pl.ds(pl.multiple_of(HALO + (k * CORES + core) * rs, HALO), rs)

    def row_copy(k):
        return remote(
            rows_in.at[spot(k), :], rows_in.at[spot(k), :], m_s.at[k], m_r.at[k], (sp, mate)
        )

    def mate_row_copy(k):
        at = pl.ds(pl.multiple_of(HALO + (k * CORES + 1 - core) * rs, HALO), rs)
        return remote(rows_in.at[at, :], rows_in.at[at, :], m_s.at[k], m_r.at[k], (sp, mate))

    def halo_copy(i, t):
        return remote(
            rows_in.at[tgt_rows : tgt_rows + HALO, :],
            rows_in.at[0:HALO, :],
            h_s.at[i],
            h_r,
            (following, t),
        )

    sends_halo = jnp.logical_and(core == 1, sp < n - 1)
    for k in reversed(range(chips)):
        at = slice(k * rs, (k + 1) * rs)
        rows_in[spot(k), :] = (res[at, :] * scale[at, :] * mgain[...]).astype(BF16)
        if k == chips - 1:

            @pl.when(sends_halo)
            def _():
                halo_copy(0, mate).start()
                halo_copy(1, tp).start()

        row_copy(k).start()

    @pl.when(sp == 0)
    def _():
        rows_in[0:HALO, :] = jnp.zeros((HALO, width), BF16)

    for k in range(chips):
        mate_row_copy(k).wait_recv()

    @pl.when(sp > 0)
    def _():
        halo_copy(0, tp).wait_recv()

    hidden_cols = hid.shape[1]
    wide = conv_g.shape[1]
    taps = gtaps.shape[0]
    for f in range(hidden_cols // wide):
        here = slice(f * wide, (f + 1) * wide)
        all_rows = rows_in[...]
        conv_g[...] = jnp.dot(all_rows, gw[:, here], preferred_element_type=F32).astype(
            BF16
        ).astype(F32)
        conv_u[...] = jnp.dot(all_rows, uw[:, here], preferred_element_type=F32).astype(
            BF16
        ).astype(F32)
        gate = jnp.zeros((tgt_rows, wide), F32)
        up = jnp.zeros((tgt_rows, wide), F32)
        for t in range(taps):
            begin = HALO - (taps - 1) + t
            gate = gate + gtaps[t : t + 1, here].astype(F32) * conv_g[begin : begin + tgt_rows, :]
            up = up + utaps[t : t + 1, here].astype(F32) * conv_u[begin : begin + tgt_rows, :]
        hid[:, here] = (gate / (1.0 + jnp.exp(-gate)) * up).astype(BF16)

    multiply_out(hid[...], dw, tail_s, tail_r, f_s, f_r)

    def end_copy(k, c):
        there = chip_at(k)
        at = pl.ds(pl.multiple_of(there * rs, rs), rs)
        return remote(
            end_s.at[c, at, :],
            end_r.at[k - 1, c],
            fx_s.at[k, c],
            fx_r.at[k, c],
            (sp, there * CORES + core),
        )

    for c in range(chunks):
        mate_wait(c, tail_s, tail_r, f_s, f_r)
        for k in range(chips):
            at = slice(k * rs, (k + 1) * rs)
            both = part[c, piece(k, core), :] + tail_r[c, at, :].astype(F32)
            part[c, piece(k, core), :] = both
            end_s[c, at, :] = both.astype(BF16)
        for k in range(1, chips):
            end_copy(k, c).start()
    own = pl.ds(pl.multiple_of(chip * rs, rs), rs)
    squares = jnp.zeros((rs, 1), F32)
    sums = []
    for c in range(chunks):
        here = slice(c * cols, (c + 1) * cols)
        total = res[own, here] + part[c, piece(chip, core), :]
        for k in range(1, chips):
            end_copy(k, c).wait_recv()
            total = total + end_r[k - 1, c].astype(F32)
        squares = squares + jnp.sum(total * total, axis=-1, keepdims=True)
        sums.append(total)
    scale = lax.rsqrt(squares / width + EPS)
    for c in range(chunks):
        here = slice(c * cols, (c + 1) * cols)
        out_ref[:, here] = (sums[c] * scale * fgain[:, here]).astype(BF16)

    for j in range(sub, runs):
        chip_copy(j).wait_send()
    for k in range(1, chips):
        for c in range(chunks):
            wide_copy(k, c).wait_send()
            end_copy(k, c).wait_send()
    for c in range(chunks):
        remote(half_s.at[c], half_r.at[c], b_s.at[c], b_r.at[c], (sp, mate)).wait_send()
        remote(tail_s.at[c], tail_r.at[c], f_s.at[c], f_r.at[c], (sp, mate)).wait_send()
    for k in range(chips):
        row_copy(k).wait_send()

    @pl.when(sends_halo)
    def _():
        halo_copy(0, mate).wait_send()
        halo_copy(1, tp).wait_send()

    def drain(d, carry):
        for j in every:
            cw_copy(d, j).wait_send()
            cc_copy(d, j).wait_send()
        return carry

    def drain_mate(slot, carry):
        for j in every:
            mate_copy(slot, j).wait_send()
        return carry

    if full >= 1:
        drain(1, 0)
    if full >= 2:
        lax.fori_loop(2, full + 1, drain, 0)
    if last:
        for j in every:
            (cw_copy if j in half_cw else cc_copy)(last, j).wait_send()
    lax.fori_loop(0, n, drain_mate, 0)


def solution(mesh):
    n = mesh.shape["sp"]
    chips = mesh.shape["tp"] // CORES
    head = 256

    def shards(*args):
        args = [a[None, :] if a.ndim == 1 else a for a in args]
        (target, source, _, _, qw, kw, _, ow, _, gw, _, _, _, dw, _) = args
        tgt_rows, width = target.shape
        r = source.shape[0]
        kv_heads = kw.shape[1] // head
        heads_here = qw.shape[1] // head
        rs = tgt_rows // (CORES * chips)
        half = chips * rs
        cols = width // 2
        chunks = width // cols
        ff = gw.shape[1]
        wide = 256 if ff % 256 == 0 else 128
        q_rows = heads_here * tgt_rows
        dists = n // 2 + 1
        sub = max(r // RUN, 1)
        runs = chips * sub
        dma = pltpu.SemaphoreType.DMA
        scratch = [pltpu.VMEM(a.shape, a.dtype) for a in args]
        scratch += [
            pltpu.VMEM((kv_heads, r, 2 * head), BF16),
            pltpu.VMEM((n * CORES * chips * r, 2 * head), BF16),
            pltpu.VMEM((q_rows, head), BF16),
            pltpu.VMEM((q_rows, 1), F32),
            pltpu.VMEM((q_rows, 1), F32),
            pltpu.VMEM((q_rows, head), F32),
            pltpu.VMEM((tgt_rows, heads_here * head), BF16),
            pltpu.VMEM((chunks, tgt_rows, cols), F32),
            pltpu.VMEM((chunks, half, cols), BF16),
            pltpu.VMEM((chunks, half, cols), BF16),
            pltpu.VMEM((chunks, half, cols), BF16),
            pltpu.VMEM((max(chips - 1, 1), chunks, half, cols), BF16),
            pltpu.VMEM((half, width), F32),
            pltpu.VMEM((HALO + tgt_rows, width), BF16),
            pltpu.VMEM((HALO + tgt_rows, wide), F32),
            pltpu.VMEM((HALO + tgt_rows, wide), F32),
            pltpu.VMEM((tgt_rows, ff), BF16),
            pltpu.VMEM((chunks, half, cols), BF16),
            pltpu.VMEM((chunks, half, cols), BF16),
            pltpu.VMEM((chunks, half, cols), BF16),
            pltpu.VMEM((max(chips - 1, 1), chunks, rs, cols), BF16),
            dma((len(args) + 2 * kv_heads,)),
            dma((runs,)),
            dma((runs,)),
        ]
        scratch += [dma((dists, runs))] * 4
        scratch += [dma((n, runs))] * 2
        scratch += [dma((chunks,))] * 2
        scratch += [dma((chips, chunks))] * 2
        scratch += [dma((chips,))] * 2
        scratch += [dma((2,)), dma]
        scratch += [dma((chunks,))] * 2
        scratch += [dma((chips, chunks))] * 2
        return pl.pallas_call(
            functools.partial(layer, (n, chips, kv_heads, head, heads_here, cols, sub)),
            out_shape=pltpu.VMEM((rs, width), BF16),
            in_specs=[pl.BlockSpec(memory_space=pl.ANY)] * len(args),
            out_specs=pl.BlockSpec(memory_space=pltpu.VMEM),
            scratch_shapes=scratch,
            compiler_params=pltpu.CompilerParams(
                collective_id=0, has_side_effects=True, vmem_limit_bytes=60 * 1024 * 1024
            ),
        )(*args)

    in_specs = (
        P("sp", None),
        P(("sp", "tp"), None),
        P(),
        P(),
        P(None, "tp"),
        P(),
        P(),
        P("tp", None),
        P(),
        P(None, "tp"),
        P(None, "tp"),
        P(None, "tp"),
        P(None, "tp"),
        P("tp", None),
        P(),
    )
    return jax.shard_map(
        shards, mesh=mesh, in_specs=in_specs, out_specs=P(("sp", "tp"), None), check_vma=False
    )
```

profile of v0, /device:TPU:0, one launch (start us, length us, event | category | flops | bytes accessed | tf_op | source)
XLA Modules:
  0.0 43.5 jit_solution(9748488057537774224)
XLA Ops:
  0.0 42.8 %shard_map.145 = bf16[32,2048]{1,0:T(8,128)(2,1)S(1)} custom-call(bf16[128,2048]{1,0:T(8,128)(2,1)} %target_h.1, bf16[64,2048]{1,0:T(8,128)(2,1)} %source_h.1, f32[1,2048]{1,0:T(1,128)} %bitcast.4, f32[1,2048]{1,0:T(1,128)} %bitcast.5, bf16[2048,512]{1,0:T(8,128)(2,1)} %qw_h.1, bf16[2048,512]{1,0:T(8,128)(2,1)} %kw_h.1, bf16[2048,512]{1,0:T(8,128)(2,1)} %vw_h.1, ...), custom_call_target="tpu_custom_call" | custom-call | tf_op jit(solution)/shard_map/pallas_call | solution.py:597
  42.8 0.7 %copy.17 = bf16[32,2048]{1,0:T(8,128)(2,1)} copy(bf16[32,2048]{1,0:T(8,128)(2,1)S(1)} %shard_map.145) | data formatting | bytes 262144
where the time goes:
time: 43.6 us; the launch traced here: 43.5 us
  Pallas kernels  42.8 us (98%)
  local copies, waits for them, and re-layouts  0.66 us (2%)
    pallas_call x1, Pallas kernels, shards(): pl.pallas_call(functools.partial(layer, (n, chips, kv_heads, head, heads_...  42.8 us

commit v1 on v0

--- a/solution.py
+++ b/solution.py
@@ -67,8 +67,12 @@
     half_r,
     chip_s,
     chip_r,
+    own_t,
     res,
     rows_in,
+    row_scale,
+    halo_s,
+    halo_r,
     conv_g,
     conv_u,
     hid,
@@ -79,10 +83,8 @@
     load_sem,
     kx_s,
     kx_r,
-    cw_s,
-    cw_r,
-    cc_s,
-    cc_r,
+    ring_s,
+    ring_r,
     d2_s,
     d2_r,
     b_s,
@@ -91,6 +93,8 @@
     bx_r,
     m_s,
     m_r,
+    rs_s,
+    rs_r,
     h_s,
     h_r,
     f_s,
@@ -98,7 +102,7 @@
     fx_s,
     fx_r,
 ):
-    n, chips, kv_heads, head, heads_here, cols, sub = dims
+    n, chips, kv_heads, head, heads_here, cols, sub, wide = dims
     tgt_rows, width = tgt.shape
     r = src.shape[0]
     rs = tgt_rows // (CORES * chips)
@@ -179,7 +183,7 @@
         there = chip_at(j // sub)
         return remote(
             kvh.at[head_of(there), (j % sub) * run : (j % sub + 1) * run, :],
-            block(0, 0, j),
+            block(0, core, j),
             kx_s.at[j],
             kx_r.at[j],
             (sp, there * CORES + core),
@@ -187,41 +191,67 @@
 
     last = n // 2 if n % 2 == 0 else 0
     full = (n - 1) // 2
-    if sub > 1:
-        half_cw = [j for j in range(runs) if j % sub < sub // 2]
-    else:
-        half_cw = list(range((runs + 1) // 2))
-    half_cc = [j for j in range(runs) if j not in half_cw]
-
-    def cw_slot(d):
-        return 2 * d - 1
-
-    def cc_slot(d):
-        return n - 1 if isinstance(d, int) and d == last else 2 * d
-
-    def cw_copy(d, j):
-        held = 0 if isinstance(d, int) and d == 1 else cw_slot(d - 1)
+    own = range(sub)
+    far = range(sub, runs)
+    onward = ahead * (1 - core) + behind * core
+
+    def slot_of(d, side):
+        if isinstance(d, int) and d == 0:
+            return 0
+        if isinstance(d, int) and d == last:
+            return n - 1
+        return 2 * d - 1 + side
+
+    def ring_copy(d, rel, j):
+        lineage = core * (1 - rel) + (1 - core) * rel
         return remote(
-            block(held, 0, j), block(cw_slot(d), 0, j), cw_s.at[d, j], cw_r.at[d, j], (ahead, tp)
+            block(slot_of(d - 1, core), lineage, j),
+            block(slot_of(d, core), lineage, j),
+            ring_s.at[d, rel, j],
+            ring_r.at[d, rel, j],
+            (onward, tp),
         )
 
-    def cc_copy(d, j):
-        held = 0 if isinstance(d, int) and d == 1 else 2 * (d - 1)
-        return remote(
-            block(held, 0, j), block(cc_slot(d), 0, j), cc_s.at[d, j], cc_r.at[d, j], (behind, tp)
-        )
-
-    def mate_copy(slot, j):
-        return remote(
-            block(slot, 0, j), block(slot, 1, j), d2_s.at[slot, j], d2_r.at[slot, j], (sp, mate)
-        )
+    def mirror_copy(d, rel, j, side):
+        lineage = side * (1 - rel) + (1 - side) * rel
+        held = block(slot_of(d, side), lineage, j)
+        return remote(held, held, d2_s.at[d, rel, j], d2_r.at[d, rel, j], (sp, mate))
+
+    def mirror_out(d, rel, j):
+        return mirror_copy(d, rel, j, core)
+
+    def mirror_in(d, rel, j):
+        return mirror_copy(d, rel, j, 1 - core)
 
     def launch(j):
-        if n > 2 or j in half_cw:
-            cw_copy(1, j).start()
-        if n > 2 or j in half_cc:
-            cc_copy(1, j).start()
-        mate_copy(0, j).start()
+        if n > 1:
+            ring_copy(1, 0, j).start()
+        mirror_out(0, 0, j).start()
+
+    def launch_mate(blocks):
+        for j in blocks:
+            mirror_in(0, 0, j).wait_recv()
+            if full >= 1:
+                ring_copy(1, 1, j).start()
+
+    def launch_far():
+        for j in far:
+            chip_copy(j).wait_recv()
+            launch(j)
+
+    def arrive(d, rel, blocks):
+        end = isinstance(d, int) and d == full
+        for j in blocks:
+            ring_copy(d, rel, j).wait_recv()
+            if not end or (last and rel == 0):
+                ring_copy(d + 1, rel, j).start()
+            mirror_out(d, rel, j).start()
+
+    def arrive_last(blocks):
+        if last:
+            for j in blocks:
+                ring_copy(last, 0, j).wait_recv()
+                mirror_out(last, 0, j).start()
 
     for copy in first:
         copy.wait()
@@ -242,25 +272,9 @@
             pl.semaphore_wait(barrier, len(peers))
             for j in range(sub, runs):
                 chip_copy(j).start()
-    kv[0:r, :] = kvh[own_head]
+    kv[pl.ds(pl.multiple_of(core * chips * r, r), r), :] = kvh[own_head]
     for j in range(sub):
         launch(j)
-    rest = [
-        load(used + 3 + i, a, b)
-        for i, (a, b) in enumerate(
-            (
-                (ow_h, ow),
-                (mgain_h, mgain),
-                (gw_h, gw),
-                (uw_h, uw),
-                (gtaps_h, gtaps),
-                (utaps_h, utaps),
-                (dw_h, dw),
-                (fgain_h, fgain),
-            )
-        )
-    ]
-
     for copy in second:
         copy.wait()
     queries = jnp.dot(normed(tgt[...], qgain[...]), qw[...], preferred_element_type=F32).astype(
@@ -268,13 +282,12 @@
     )
     for h in range(heads_here):
         q2[h * tgt_rows : (h + 1) * tgt_rows, :] = queries[:, h * head : (h + 1) * head]
+    for k in range(chips):
+        at = pl.ds(pl.multiple_of((k * CORES + core) * rs, rs), rs)
+        own_t[k * rs : (k + 1) * rs, :] = tgt[at, :]
     top[...] = jnp.full(top.shape, -1e30, F32)
     tot[...] = jnp.zeros(tot.shape, F32)
     acc[...] = jnp.zeros(acc.shape, F32)
-
-    for j in range(sub, runs):
-        chip_copy(j).wait_recv()
-        launch(j)
 
     slot_rows = CORES * chips * r
 
@@ -282,9 +295,6 @@
         start = slot * slot_rows
         if not isinstance(start, int):
             start = pl.multiple_of(start, slot_rows)
-        for s in range(slots):
-            for j in range(runs):
-                mate_copy(slot + s, j).wait_recv()
         here = pl.ds(start, slots * slot_rows)
         scores = lax.dot_general(
             q2[...], kv[here, :head], (((1,), (1,)), ((), ())), preferred_element_type=F32
@@ -299,47 +309,82 @@
             probs.astype(BF16), kv[here, head:], preferred_element_type=F32
         )
 
-    def step(d, cw_on, cc_on):
-        for j in range(runs):
-            cw_copy(d, j).wait_recv()
-            if j in cw_on:
-                cw_copy(d + 1, j).start()
-            mate_copy(cw_slot(d), j).start()
-            cc_copy(d, j).wait_recv()
-            if j in cc_on:
-                cc_copy(d + 1, j).start()
-            mate_copy(cc_slot(d), j).start()
-
-    every = range(runs)
-    few = half_cw if last else []
-    others = half_cc if last else []
+    def mirrored(d):
+        for rel in range(1 if isinstance(d, int) and d == last else CORES):
+            for j in range(runs):
+                mirror_in(d, rel, j).wait_recv()
+
+    def wave(d):
+        for blocks in (own, far):
+            for rel in range(CORES):
+                arrive(d, rel, blocks)
+
     if full >= 1:
-        step(1, every if full > 1 else few, every if full > 1 else others)
+        launch_mate(own)
+        launch_far()
+        launch_mate(far)
+        wave(1)
+        rest = [
+            load(used + 3 + i, a, b)
+            for i, (a, b) in enumerate(
+                (
+                    (ow_h, ow),
+                    (mgain_h, mgain),
+                    (gw_h, gw),
+                    (uw_h, uw),
+                    (gtaps_h, gtaps),
+                    (utaps_h, utaps),
+                    (dw_h, dw),
+                    (fgain_h, fgain),
+                )
+            )
+        ]
+        done = 1
+        if full > 4:
+            wave(2)
+            attend(0, 1)
+
+            def middle(d, carry):
+                wave(d)
+                mirrored(d - 2)
+                attend(2 * d - 5, 2)
+                return carry
+
+            lax.fori_loop(3, full, middle, 0)
+            wave(full)
+            done = full - 2
+        else:
+            for d in range(2, full + 1):
+                wave(d)
+        start = 2 * done - 1 if full > 4 else 0
+        for d in range(done, full):
+            mirrored(d)
+        attend(start, 2 * full - 1 - start)
+        arrive_last(range(runs))
+        mirrored(full)
+        attend(2 * full - 1, 2)
+    else:
+        rest = [
+            load(used + 3 + i, a, b)
+            for i, (a, b) in enumerate(
+                (
+                    (ow_h, ow),
+                    (mgain_h, mgain),
+                    (gw_h, gw),
+                    (uw_h, uw),
+                    (gtaps_h, gtaps),
+                    (utaps_h, utaps),
+                    (dw_h, dw),
+                    (fgain_h, fgain),
+                )
+            )
+        ]
+        launch_far()
+        launch_mate(range(runs))
+        arrive_last(range(runs))
         attend(0, 1)
-        if full > 6:
-
-            def middle(d, carry):
-                step(d, every, every)
-                attend(2 * d - 3, 2)
-                return carry
-
-            lax.fori_loop(2, full, middle, 0)
-        else:
-            for d in range(2, full):
-                step(d, every, every)
-                attend(2 * d - 3, 2)
-        if full > 1:
-            step(full, few, others)
-            attend(2 * full - 3, 2)
-        tail_slot, tail_count = 2 * full - 1, 2
-    else:
-        tail_slot, tail_count = 0, 1
     if last:
-        for j in every:
-            (cw_copy if j in half_cw else cc_copy)(last, j).wait_recv()
-            mate_copy(n - 1, j).start()
-    attend(tail_slot, tail_count)
-    if last:
+        mirrored(last)
         attend(n - 1, 1)
 
     attended = (acc[...] / tot[...]).astype(BF16)
@@ -364,100 +409,132 @@
 
     multiply_out(att[...], ow, half_s, half_r, b_s, b_r)
 
-    def wide_copy(k, c):
+    body_rows = half_rows - HALO
+    body = slice(0, body_rows)
+    tail = slice(body_rows, half_rows)
+
+    def wide_copy(k, c, i):
+        at = (body, tail)[i]
         return remote(
-            chip_s.at[c],
-            chip_r.at[k - 1, c],
-            bx_s.at[k, c],
-            bx_r.at[k, c],
+            chip_s.at[c, at, :],
+            chip_r.at[k - 1, c, at, :],
+            bx_s.at[k, c, i],
+            bx_r.at[k, c, i],
             (sp, chip_at(k) * CORES + core),
         )
 
     for c in range(chunks):
         mate_wait(c, half_s, half_r, b_s, b_r)
+        here = slice(c * cols, (c + 1) * cols)
         for k in range(chips):
             at = slice(k * rs, (k + 1) * rs)
             both = part[c, piece(k, core), :] + half_r[c, at, :].astype(F32)
-            res[at, c * cols : (c + 1) * cols] = both
+            res[at, here] = both + own_t[at, here].astype(F32)
             chip_s[c, at, :] = both.astype(BF16)
         for k in range(1, chips):
-            wide_copy(k, c).start()
-    squares = jnp.zeros((half_rows, 1), F32)
+            wide_copy(k, c, 1).start()
+    for c in range(chunks):
+        for k in range(1, chips):
+            wide_copy(k, c, 0).start()
+
+    def settle(c, i):
+        at = (body, tail)[i]
+        here = slice(c * cols, (c + 1) * cols)
+        residual = res[at, here]
+        for k in range(1, chips):
+            wide_copy(k, c, i).wait_recv()
+            residual = residual + chip_r[k - 1, c, at, :].astype(F32)
+        residual = residual.astype(BF16).astype(F32)
+        res[at, here] = residual
+        return jnp.sum(residual * residual, axis=-1, keepdims=True)
+
+    def spot(k, side):
+        return pl.ds(pl.multiple_of((k * CORES + side) * rs, rs), rs)
+
+    def row_copy(c, k, side):
+        held = rows_in.at[c, spot(k, side), :]
+        return remote(held, held, m_s.at[c, k], m_r.at[c, k], (sp, mate))
+
+    def scale_copy(k, side):
+        held = row_scale.at[spot(k, side), :]
+        return remote(held, held, rs_s.at[k], rs_r.at[k], (sp, mate))
+
+    def halo_copy(i, t):
+        return remote(halo_s, halo_r, h_s.at[i], h_r, (following, t))
+
+    sends_halo = jnp.logical_and(core == 1, sp < n - 1)
+    tail_squares = settle(0, 1)
+    for c in range(1, chunks):
+        tail_squares = tail_squares + settle(c, 1)
+    scale = lax.rsqrt(tail_squares / width + EPS)
     for c in range(chunks):
         here = slice(c * cols, (c + 1) * cols)
-        projected = res[:, here]
-        for k in range(1, chips):
-            wide_copy(k, c).wait_recv()
-            projected = projected + chip_r[k - 1, c].astype(F32)
-        mine = jnp.concatenate([tgt[piece(k, core), here] for k in range(chips)], axis=0)
-        residual = (mine.astype(F32) + projected).astype(BF16).astype(F32)
-        res[:, here] = residual
-        squares = squares + jnp.sum(residual * residual, axis=-1, keepdims=True)
-    scale = lax.rsqrt(squares / width + EPS)
-
-    def spot(k):
-        return pl.ds(pl.multiple_of(HALO + (k * CORES + core) * rs, HALO), rs)
-
-    def row_copy(k):
-        return remote(
-            rows_in.at[spot(k), :], rows_in.at[spot(k), :], m_s.at[k], m_r.at[k], (sp, mate)
-        )
-
-    def mate_row_copy(k):
-        at = pl.ds(pl.multiple_of(HALO + (k * CORES + 1 - core) * rs, HALO), rs)
-        return remote(rows_in.at[at, :], rows_in.at[at, :], m_s.at[k], m_r.at[k], (sp, mate))
-
-    def halo_copy(i, t):
-        return remote(
-            rows_in.at[tgt_rows : tgt_rows + HALO, :],
-            rows_in.at[0:HALO, :],
-            h_s.at[i],
-            h_r,
-            (following, t),
-        )
-
-    sends_halo = jnp.logical_and(core == 1, sp < n - 1)
-    for k in reversed(range(chips)):
-        at = slice(k * rs, (k + 1) * rs)
-        rows_in[spot(k), :] = (res[at, :] * scale[at, :] * mgain[...]).astype(BF16)
-        if k == chips - 1:
-
-            @pl.when(sends_halo)
-            def _():
-                halo_copy(0, mate).start()
-                halo_copy(1, tp).start()
-
-        row_copy(k).start()
+        halo_s[c] = (res[tail, here] * scale * mgain[:, here]).astype(BF16)
+
+    @pl.when(sends_halo)
+    def _():
+        halo_copy(0, mate).start()
+        halo_copy(1, tp).start()
+
+    def mix(c):
+        for k in range(chips):
+            row_copy(c, k, 1 - core).wait_recv()
+        here = slice(c * cols, (c + 1) * cols)
+        for weight, total in ((gw, conv_g), (uw, conv_u)):
+            product = jnp.dot(rows_in[c], weight[here, :], preferred_element_type=F32)
+            if c > 0:
+                product = product + total[HALO:, :]
+            total[HALO:, :] = product
+
+    squares = jnp.zeros((body_rows, 1), F32)
+    for c in range(chunks):
+        squares = squares + settle(c, 0)
+        here = slice(c * cols, (c + 1) * cols)
+        for k in range(chips):
+            at = slice(k * rs, (k + 1) * rs)
+            rows_in[c, spot(k, core), :] = (res[at, here] * mgain[:, here]).astype(BF16)
+            row_copy(c, k, core).start()
+        if c > 0:
+            mix(c - 1)
+    squares = jnp.concatenate([squares, tail_squares], axis=0)
+    scale = jnp.broadcast_to(lax.rsqrt(squares / width + EPS), (half_rows, row_scale.shape[1]))
+    for k in range(chips):
+        row_scale[spot(k, core), :] = scale[k * rs : (k + 1) * rs, :]
+        scale_copy(k, core).start()
 
     @pl.when(sp == 0)
     def _():
-        rows_in[0:HALO, :] = jnp.zeros((HALO, width), BF16)
-
-    for k in range(chips):
-        mate_row_copy(k).wait_recv()
+        halo_r[...] = jnp.zeros(halo_r.shape, BF16)
 
     @pl.when(sp > 0)
     def _():
         halo_copy(0, tp).wait_recv()
 
+    for weight, total in ((gw, conv_g), (uw, conv_u)):
+        product = jnp.zeros((HALO, weight.shape[1]), F32)
+        for c in range(chunks):
+            product = product + jnp.dot(
+                halo_r[c], weight[c * cols : (c + 1) * cols, :], preferred_element_type=F32
+            )
+        total[:HALO, :] = product.astype(BF16).astype(F32)
+    mix(chunks - 1)
+    for k in range(chips):
+        scale_copy(k, 1 - core).wait_recv()
+
     hidden_cols = hid.shape[1]
-    wide = conv_g.shape[1]
     taps = gtaps.shape[0]
     for f in range(hidden_cols // wide):
         here = slice(f * wide, (f + 1) * wide)
-        all_rows = rows_in[...]
-        conv_g[...] = jnp.dot(all_rows, gw[:, here], preferred_element_type=F32).astype(
-            BF16
-        ).astype(F32)
-        conv_u[...] = jnp.dot(all_rows, uw[:, here], preferred_element_type=F32).astype(
-            BF16
-        ).astype(F32)
+        scale = row_scale[:, :1]
+        for total in (conv_g, conv_u):
+            total[HALO:, here] = (total[HALO:, here] * scale).astype(BF16).astype(F32)
         gate = jnp.zeros((tgt_rows, wide), F32)
         up = jnp.zeros((tgt_rows, wide), F32)
         for t in range(taps):
             begin = HALO - (taps - 1) + t
-            gate = gate + gtaps[t : t + 1, here].astype(F32) * conv_g[begin : begin + tgt_rows, :]
-            up = up + utaps[t : t + 1, here].astype(F32) * conv_u[begin : begin + tgt_rows, :]
+            rows = slice(begin, begin + tgt_rows)
+            gate = gate + gtaps[t : t + 1, here].astype(F32) * conv_g[rows, here]
+            up = up + utaps[t : t + 1, here].astype(F32) * conv_u[rows, here]
         hid[:, here] = (gate / (1.0 + jnp.exp(-gate)) * up).astype(BF16)
 
     multiply_out(hid[...], dw, tail_s, tail_r, f_s, f_r)
@@ -502,13 +579,16 @@
         chip_copy(j).wait_send()
     for k in range(1, chips):
         for c in range(chunks):
-            wide_copy(k, c).wait_send()
+            wide_copy(k, c, 0).wait_send()
+            wide_copy(k, c, 1).wait_send()
             end_copy(k, c).wait_send()
     for c in range(chunks):
         remote(half_s.at[c], half_r.at[c], b_s.at[c], b_r.at[c], (sp, mate)).wait_send()
         remote(tail_s.at[c], tail_r.at[c], f_s.at[c], f_r.at[c], (sp, mate)).wait_send()
     for k in range(chips):
-        row_copy(k).wait_send()
+        scale_copy(k, core).wait_send()
+        for c in range(chunks):
+            row_copy(c, k, core).wait_send()
 
     @pl.when(sends_halo)
     def _():
@@ -516,24 +596,20 @@
         halo_copy(1, tp).wait_send()
 
     def drain(d, carry):
-        for j in every:
-            cw_copy(d, j).wait_send()
-            cc_copy(d, j).wait_send()
+        for rel in range(1 if isinstance(d, int) and d in (0, last) else CORES):
+            for j in range(runs):
+                if not isinstance(d, int) or d > 0:
+                    ring_copy(d, rel, j).wait_send()
+                mirror_out(d, rel, j).wait_send()
         return carry
 
-    def drain_mate(slot, carry):
-        for j in every:
-            mate_copy(slot, j).wait_send()
-        return carry
-
+    drain(0, 0)
     if full >= 1:
         drain(1, 0)
     if full >= 2:
         lax.fori_loop(2, full + 1, drain, 0)
     if last:
-        for j in every:
-            (cw_copy if j in half_cw else cc_copy)(last, j).wait_send()
-    lax.fori_loop(0, n, drain_mate, 0)
+        drain(last, 0)
 
 
 def solution(mesh):
@@ -550,7 +626,7 @@
         heads_here = qw.shape[1] // head
         rs = tgt_rows // (CORES * chips)
         half = chips * rs
-        cols = width // 2
+        cols = width // 4
         chunks = width // cols
         ff = gw.shape[1]
         wide = 256 if ff % 256 == 0 else 128
@@ -573,10 +649,14 @@
             pltpu.VMEM((chunks, half, cols), BF16),
             pltpu.VMEM((chunks, half, cols), BF16),
             pltpu.VMEM((max(chips - 1, 1), chunks, half, cols), BF16),
+            pltpu.VMEM((half, width), BF16),
             pltpu.VMEM((half, width), F32),
-            pltpu.VMEM((HALO + tgt_rows, width), BF16),
-            pltpu.VMEM((HALO + tgt_rows, wide), F32),
-            pltpu.VMEM((HALO + tgt_rows, wide), F32),
+            pltpu.VMEM((chunks, tgt_rows, cols), BF16),
+            pltpu.VMEM((tgt_rows, 128), F32),
+            pltpu.VMEM((chunks, HALO, cols), BF16),
+            pltpu.VMEM((chunks, HALO, cols), BF16),
+            pltpu.VMEM((HALO + tgt_rows, ff), F32),
+            pltpu.VMEM((HALO + tgt_rows, ff), F32),
             pltpu.VMEM((tgt_rows, ff), BF16),
             pltpu.VMEM((chunks, half, cols), BF16),
             pltpu.VMEM((chunks, half, cols), BF16),
@@ -586,16 +666,16 @@
             dma((runs,)),
             dma((runs,)),
         ]
-        scratch += [dma((dists, runs))] * 4
-        scratch += [dma((n, runs))] * 2
+        scratch += [dma((dists, CORES, runs))] * 4
         scratch += [dma((chunks,))] * 2
-        scratch += [dma((chips, chunks))] * 2
+        scratch += [dma((chips, chunks, 2))] * 2
+        scratch += [dma((chunks, chips))] * 2
         scratch += [dma((chips,))] * 2
         scratch += [dma((2,)), dma]
         scratch += [dma((chunks,))] * 2
         scratch += [dma((chips, chunks))] * 2
         return pl.pallas_call(
-            functools.partial(layer, (n, chips, kv_heads, head, heads_here, cols, sub)),
+            functools.partial(layer, (n, chips, kv_heads, head, heads_here, cols, sub, wide)),
             out_shape=pltpu.VMEM((rs, width), BF16),
             in_specs=[pl.BlockSpec(memory_space=pl.ANY)] * len(args),
             out_specs=pl.BlockSpec(memory_space=pltpu.VMEM),

time: 43.6 us -> 44.3 us (1.016)
  Pallas kernels: 42.8 us -> 43.5 us
    pallas_call x1, Pallas kernels: 42.8 us -> 43.5 us  [shards(): pl.pallas_call(functools.partial(layer, (n, chips, kv_heads, head, heads_...]
where the time goes in v1:
time: 44.3 us; the launch traced here: 44.1 us
  Pallas kernels  43.5 us (98%)
  local copies, waits for them, and re-layouts  0.66 us (1%)
    pallas_call x1, Pallas kernels, shards(): pl.pallas_call(functools.partial(layer, (n, chips, kv_heads, head, heads_...  43.5 us

profile of v1, /device:TPU:0, one launch (start us, length us, event | category | flops | bytes accessed | tf_op | source)
XLA Modules:
  0.0 44.1 jit_solution(11597277864573931595)
XLA Ops:
  0.0 43.5 %shard_map.145 = bf16[32,2048]{1,0:T(8,128)(2,1)S(1)} custom-call(bf16[128,2048]{1,0:T(8,128)(2,1)} %target_h.1, bf16[64,2048]{1,0:T(8,128)(2,1)} %source_h.1, f32[1,2048]{1,0:T(1,128)} %bitcast.4, f32[1,2048]{1,0:T(1,128)} %bitcast.5, bf16[2048,512]{1,0:T(8,128)(2,1)} %qw_h.1, bf16[2048,512]{1,0:T(8,128)(2,1)} %kw_h.1, bf16[2048,512]{1,0:T(8,128)(2,1)} %vw_h.1, ...), custom_call_target="tpu_custom_call" | custom-call | tf_op jit(solution)/shard_map/pallas_call | solution.py:677
  43.5 0.7 %copy.17 = bf16[32,2048]{1,0:T(8,128)(2,1)} copy(bf16[32,2048]{1,0:T(8,128)(2,1)S(1)} %shard_map.145) | data formatting | bytes 262144

commit v2 on v1

v2 whole, which is shorter than its diff:
```python
import functools

import jax
import jax.numpy as jnp
from jax import lax
from jax.experimental import pallas as pl
from jax.experimental.pallas import tpu as pltpu
from jax.sharding import PartitionSpec as P

MESH = pl.DeviceIdType.MESH
EPS = 1e-06
HALO = 16
RUN = 32
CORES = 2
SPLIT = 8
F32 = jnp.float32
BF16 = jnp.bfloat16


def normed(values, gain):
    wide = values.astype(F32)
    scale = lax.rsqrt(jnp.mean(wide * wide, axis=-1, keepdims=True) + EPS)
    return (wide * scale * gain).astype(BF16)


def layer(
    dims,
    target_h,
    source_h,
    qgain_h,
    sgain_h,
    qw_h,
    kw_h,
    vw_h,
    ow_h,
    mgain_h,
    gw_h,
    uw_h,
    gtaps_h,
    utaps_h,
    dw_h,
    fgain_h,
    out_ref,
    tgt,
    src,
    qgain,
    sgain,
    qw,
    kw,
    vw,
    ow,
    mgain,
    gw,
    uw,
    gtaps,
    utaps,
    dw,
    fgain,
    kvh,
    kv,
    q2,
    top,
    tot,
    acc,
    att,
    chip_s,
    chip_r,
    q_held,
    res,
    rows_in,
    halo_s,
    conv_g,
    conv_u,
    hid,
    end_s,
    end_r,
    kept,
    res_s,
    res_r,
    load_sem,
    kx_s,
    kx_r,
    ring_s,
    ring_r,
    d2_s,
    d2_r,
    d2_first,
    q_s,
    q_r,
    w_s,
    w_r,
    bx_s,
    bx_r,
    h_s,
    h_r,
    r_s,
    r_r,
    fx_s,
    fx_r,
):
    n, chips, kv_heads, head, heads_here, cols, sub, wide = dims
    tgt_rows, width = tgt.shape
    r = src.shape[0]
    rs = tgt_rows // (CORES * chips)
    half_rows = chips * rs
    run = r // sub
    runs = chips * sub
    chunks = width // cols
    ff = gw_h.shape[1]
    sp = lax.axis_index("sp")
    tp = lax.axis_index("tp")
    chip = tp // CORES
    core = tp % CORES
    mate = tp + 1 - 2 * core
    base = pl.multiple_of(core * half_rows, half_rows)

    def chip_at(k):
        return (chip + k) % chips

    def ring_at(p):
        if n % 2:
            return p
        upper = p // (n // 2)
        return 2 * (p * (1 - upper) + (n - 1 - p) * upper) + upper

    if n % 2:
        pos = sp
    else:
        pos = (sp // 2) * (1 - sp % 2) + (n - 1 - sp // 2) * (sp % 2)
    ahead = ring_at((pos + 1) % n)
    behind = ring_at((pos + n - 1) % n)

    def load(index, hbm, vmem):
        copy = pltpu.make_async_copy(hbm, vmem, load_sem.at[index])
        copy.start()
        return copy

    def head_of(c):
        return (c * CORES * kv_heads) // (chips * CORES)

    own_head = head_of(chip)
    order = [(own_head + 1 + g) % kv_heads for g in range(kv_heads)]

    def columns(g):
        return pl.ds(pl.multiple_of(g * head, head), head)

    first = [load(0, source_h, src), load(1, sgain_h, sgain)]
    by_head = [
        [
            load(2 + 2 * i, kw_h.at[:, columns(g)], kw.at[:, columns(g)]),
            load(3 + 2 * i, vw_h.at[:, columns(g)], vw.at[:, columns(g)]),
        ]
        for i, g in enumerate(order)
    ]
    used = 2 + 2 * kv_heads

    barrier = pltpu.get_barrier_semaphore()
    following = (sp + 1) % n
    peers = [(ahead, tp), (behind, tp), (sp, mate)]
    peers += [(sp, chip_at(k) * CORES + core) for k in range(1, chips)]
    for peer in peers:
        pl.semaphore_signal(barrier, inc=1, device_id=peer, device_id_type=MESH)

    def remote(source_ref, dest_ref, send, recv, device):
        return pltpu.make_async_remote_copy(
            src_ref=source_ref,
            dst_ref=dest_ref,
            send_sem=send,
            recv_sem=recv,
            device_id=device,
            device_id_type=MESH,
        )

    def block(slot, lineage, j):
        start = ((slot * CORES + lineage) * runs + j) * run
        if not isinstance(start, int):
            start = pl.multiple_of(start, run)
        return kv.at[pl.ds(start, run), :]

    def chip_copy(j):
        there = chip_at(j // sub)
        return remote(
            kvh.at[head_of(there), (j % sub) * run : (j % sub + 1) * run, :],
            block(0, core, j),
            kx_s,
            kx_r.at[j - sub],
            (sp, there * CORES + core),
        )

    last = n // 2 if n % 2 == 0 else 0
    full = (n - 1) // 2
    own = range(sub)
    far = range(sub, runs)
    onward = ahead * (1 - core) + behind * core

    def slot_of(d, side):
        if isinstance(d, int) and d == 0:
            return 0
        if isinstance(d, int) and d == last:
            return n - 1
        return 2 * d - 1 + side

    def ring_copy(d, rel, j):
        lineage = core * (1 - rel) + (1 - core) * rel
        return remote(
            block(slot_of(d - 1, core), lineage, j),
            block(slot_of(d, core), lineage, j),
            ring_s,
            ring_r.at[d - 1, rel, j],
            (onward, tp),
        )

    def mirror_copy(d, rel, j, side):
        lineage = side * (1 - rel) + (1 - side) * rel
        held = block(slot_of(d, side), lineage, j)
        first = isinstance(d, int) and d == 0
        return remote(held, held, d2_s, d2_first.at[j] if first else d2_r.at[d - 1], (sp, mate))

    def mirror_out(d, rel, j):
        return mirror_copy(d, rel, j, core)

    def mirror_in(d, rel, j):
        return mirror_copy(d, rel, j, 1 - core)

    def whole(w, side):
        high = w.shape[0] // CORES
        return w.at[pl.ds(pl.multiple_of(side * high, high), high), :]

    shared = [
        (ow_h, lambda side: whole(ow, side), SPLIT),
        (gw_h, lambda side: gw.at[side], SPLIT),
        (uw_h, lambda side: uw.at[side], SPLIT),
        (gtaps_h, lambda side: gtaps.at[side], 1),
        (utaps_h, lambda side: utaps.at[side], 1),
        (dw_h, lambda side: whole(dw, side), SPLIT),
    ]

    def push(i, p, side):
        held, place, pieces = shared[i]
        high = held.shape[0] // pieces
        at = slice(p * high, (p + 1) * high)
        there = place(side)
        return remote(
            held.at[at, :], there.at[at, :], w_s.at[i], w_r.at[i], (sp, mate)
        )

    def pushed(i, side):
        held, place, _ = shared[i]
        return remote(held, place(side), w_s.at[i], w_r.at[i], (sp, mate))

    pending = [(i, p) for i in range(len(shared)) for p in range(shared[i][2])]

    def feed(count):
        for x in pending[:count]:
            push(*x, core).start()
        del pending[:count]

    def shared_wait(i):
        pushed(i, 1 - core).wait_recv()

    def launch(j):
        if n > 1:
            ring_copy(1, 0, j).start()
        mirror_out(0, 0, j).start()

    def launch_mate(blocks):
        for j in blocks:
            mirror_in(0, 0, j).wait_recv()
            if full >= 1:
                ring_copy(1, 1, j).start()

    def launch_far():
        for j in far:
            chip_copy(j).wait_recv()
            launch(j)

    quota = {1: 5, 2: 4, 3: 3}

    def arrive(d, rel, blocks):
        end = isinstance(d, int) and d == full
        for j in blocks:
            ring_copy(d, rel, j).wait_recv()
            if not end or (last and rel == 0):
                ring_copy(d + 1, rel, j).start()
            mirror_out(d, rel, j).start()
            if isinstance(d, int) and d in quota and quota[d] > 0:
                quota[d] -= 1
                feed(1)

    def arrive_last(blocks):
        if last:
            for j in blocks:
                ring_copy(last, 0, j).wait_recv()
                mirror_out(last, 0, j).start()

    for copy in first:
        copy.wait()
    source_in = normed(src[...], sgain[...])
    second = [
        load(used + i, a, b)
        for i, (a, b) in enumerate(((target_h, tgt), (qgain_h, qgain), (qw_h, qw)))
    ]
    early = chips == kv_heads
    for i, g in enumerate(order):
        for copy in by_head[i]:
            copy.wait()
        keys = jnp.dot(source_in, kw[:, columns(g)], preferred_element_type=F32)
        kvh[g, :, :head] = keys.astype(BF16)
        values = jnp.dot(source_in, vw[:, columns(g)], preferred_element_type=F32)
        kvh[g, :, head:] = values.astype(BF16)
        if i == (kv_heads - 2 if early else kv_heads - 1):
            pl.semaphore_wait(barrier, len(peers))
            for j in range(sub, runs):
                chip_copy(j).start()
    kv[pl.ds(pl.multiple_of(core * chips * r, r), r), :] = kvh[own_head]
    for j in range(sub):
        launch(j)
    for copy in second:
        copy.wait()
    queries = jnp.dot(normed(tgt[...], qgain[...]), qw[...], preferred_element_type=F32).astype(
        BF16
    )
    group = heads_here * half_rows
    for side in range(CORES):
        for h in range(heads_here):
            q_held[side, h * half_rows : (h + 1) * half_rows, :] = queries[
                side * half_rows : (side + 1) * half_rows, h * head : (h + 1) * head
            ]

    def q_copy(side):
        return remote(
            q_held.at[1 - core],
            q2.at[pl.ds(pl.multiple_of(side * group, group), group), :],
            q_s,
            q_r,
            (sp, mate),
        )

    q_copy(core).start()
    q2[pl.ds(pl.multiple_of(core * group, group), group), :] = q_held[core]
    top[...] = jnp.full(top.shape, -1e30, F32)
    tot[...] = jnp.zeros(tot.shape, F32)
    acc[...] = jnp.zeros(acc.shape, F32)

    slot_rows = CORES * chips * r

    def attend(slot, slots):
        start = slot * slot_rows
        if not isinstance(start, int):
            start = pl.multiple_of(start, slot_rows)
        here = pl.ds(start, slots * slot_rows)
        scores = lax.dot_general(
            q2[...], kv[here, :head], (((1,), (1,)), ((), ())), preferred_element_type=F32
        ) * (head**-0.5)
        old = top[...]
        new = jnp.maximum(old, jnp.max(scores, axis=-1, keepdims=True))
        shrink = jnp.exp(old - new)
        probs = jnp.exp(scores - new)
        top[...] = new
        tot[...] = tot[...] * shrink + jnp.sum(probs, axis=-1, keepdims=True)
        acc[...] = acc[...] * shrink + jnp.dot(
            probs.astype(BF16), kv[here, head:], preferred_element_type=F32
        )

    def local_loads():
        pairs = [(held, place(core)) for held, place, _ in shared]
        pairs += [(mgain_h, mgain), (fgain_h, fgain)]
        return [load(used + 3 + i, a, b) for i, (a, b) in enumerate(pairs)]

    def mirrored(d):
        end = isinstance(d, int) and d == last
        rows = slot_rows // CORES if end else slot_rows
        start = slot_of(d, 1 - core) * slot_rows
        if end:
            start = start + (1 - core) * rows
        held = kv.at[pl.ds(pl.multiple_of(start, rows), rows), :]
        remote(held, held, d2_s, d2_r.at[d - 1], (sp, mate)).wait_recv()

    def wave(d):
        for blocks in (own, far):
            for rel in range(CORES):
                arrive(d, rel, blocks)

    if full >= 1:
        feed(2)
        launch_mate(own)
        launch_far()
        feed(3)
        launch_mate(far)
        q_copy(1 - core).wait_recv()
        wave(1)
        rest = local_loads()
        done = 1
        if full > 4:
            wave(2)
            attend(0, 1)

            def middle(d, carry):
                wave(d)
                mirrored(d - 2)
                attend(2 * d - 5, 2)
                return carry

            lax.fori_loop(3, full, middle, 0)
            wave(full)
            done = full - 2
        else:
            for d in range(2, full + 1):
                wave(d)
        start = 2 * done - 1 if full > 4 else 0
        for d in range(done, full):
            mirrored(d)
        attend(start, 2 * full - 1 - start)
        arrive_last(range(runs))
        feed(len(pending) - SPLIT)
        mirrored(full)
        attend(2 * full - 1, 2)
    else:
        rest = local_loads()
        launch_far()
        launch_mate(range(runs))
        q_copy(1 - core).wait_recv()
        arrive_last(range(runs))
        feed(3 * SPLIT + 2)
        attend(0, 1)
    if last:
        mirrored(last)
        attend(n - 1, 1)

    attended = (acc[...] / tot[...]).astype(BF16)
    for h in range(CORES * heads_here):
        att[:, h * head : (h + 1) * head] = attended[h * half_rows : (h + 1) * half_rows, :]
    for copy in rest:
        copy.wait()
    shared_wait(0)

    body_rows = half_rows - HALO
    body = slice(0, body_rows)
    tail = slice(body_rows, half_rows)

    def wide_copy(k, c, i):
        at = (body, tail)[i]
        return remote(
            chip_s.at[c, at, :],
            chip_r.at[k - 1, c, at, :],
            bx_s.at[k],
            bx_r.at[k, c * (1 - i) + chunks * i],
            (sp, chip_at(k) * CORES + core),
        )

    for c in range(chunks):
        here = slice(c * cols, (c + 1) * cols)
        product = jnp.dot(att[...], ow[:, here], preferred_element_type=F32)
        chip_s[c] = product.astype(BF16)
        for k in range(1, chips):
            wide_copy(k, c, 1).start()
        res[:, here] = product + tgt[pl.ds(base, half_rows), here].astype(F32)
    for c in range(chunks):
        for k in range(1, chips):
            wide_copy(k, c, 0).start()

    def wide_all(k, at, recv):
        return remote(
            chip_s.at[:, at, :],
            chip_r.at[k - 1, :, at, :],
            bx_s.at[k],
            bx_r.at[k, recv],
            (sp, chip_at(k) * CORES + core),
        )

    def settle(c, i):
        at = (body, tail)[i]
        here = slice(c * cols, (c + 1) * cols)
        residual = res[at, here]
        for k in range(1, chips):
            if i == 0:
                wide_copy(k, c, 0).wait_recv()
            residual = residual + chip_r[k - 1, c, at, :].astype(F32)
        residual = residual.astype(BF16).astype(F32)
        res[at, here] = residual
        return jnp.sum(residual * residual, axis=-1, keepdims=True)

    for k in range(1, chips):
        wide_all(k, tail, chunks).wait_recv()

    beyond = sp * (1 - core) + following * core

    halo = remote(halo_s, rows_in.at[:, 0:HALO, :], h_s, h_r, (beyond, mate))

    sends_halo = jnp.logical_or(core == 0, sp < n - 1)
    takes_halo = jnp.logical_or(core == 1, sp > 0)
    tail_squares = settle(0, 1)
    for c in range(1, chunks):
        tail_squares = tail_squares + settle(c, 1)
    scale = lax.rsqrt(tail_squares / width + EPS)
    for c in range(chunks):
        here = slice(c * cols, (c + 1) * cols)
        halo_s[c] = (res[tail, here] * scale * mgain[:, here]).astype(BF16)

    @pl.when(sends_halo)
    def _():
        halo.start()

    feed(len(pending))

    @pl.when(jnp.logical_not(takes_halo))
    def _():
        rows_in[:, 0:HALO, :] = jnp.zeros((chunks, HALO, cols), BF16)

    def ready():
        @pl.when(takes_halo)
        def _():
            halo.wait_recv()

    def mix(c):
        here = slice(c * cols, (c + 1) * cols)
        for side in range(CORES):
            there = slice(side * ff, (side + 1) * ff)
            for weight, total in ((gw, conv_g), (uw, conv_u)):
                product = jnp.dot(
                    rows_in[c], weight[side, here, :], preferred_element_type=F32
                )
                if c > 0:
                    product = product + total[:, there]
                total[:, there] = product

    for i in range(1, len(shared) - 1):
        shared_wait(i)
    squares = jnp.zeros((body_rows, 1), F32)
    for c in range(chunks):
        squares = squares + settle(c, 0)
        here = slice(c * cols, (c + 1) * cols)
        rows_in[c, HALO:, :] = (res[:, here] * mgain[:, here]).astype(BF16)
        if c == chunks - 2:
            ready()
            for i in range(chunks - 1):
                mix(i)
    squares = jnp.concatenate([squares, tail_squares], axis=0)
    scale = jnp.concatenate(
        [jnp.ones((HALO, 1), F32), lax.rsqrt(squares / width + EPS)], axis=0
    )

    from_core = tp // chips
    held_row = pl.multiple_of((tp % chips) * rs, rs)
    mate_row = pl.multiple_of((mate % chips) * rs, rs)
    sends_res = mate // chips == core
    holds = from_core == core

    def res_copy():
        return remote(res_s, res_r, r_s, r_r, (sp, mate))

    @pl.when(sends_res)
    def _():
        res_s[...] = res[pl.ds(mate_row, rs), :].astype(BF16)
        res_copy().start()

    taps = gtaps.shape[1]
    last_rows = slice((chunks - 1) * cols, chunks * cols)
    blocks_here = ff // wide
    for f in range(CORES * blocks_here):
        side = f // blocks_here
        part = slice((f % blocks_here) * wide, (f % blocks_here + 1) * wide)
        here = slice(f * wide, (f + 1) * wide)
        for weight, total in ((gw, conv_g), (uw, conv_u)):
            product = total[:, here] + jnp.dot(
                rows_in[chunks - 1], weight[side, last_rows, part], preferred_element_type=F32
            )
            total[:, here] = (product * scale).astype(BF16).astype(F32)
        gate = jnp.zeros((half_rows, wide), F32)
        up = jnp.zeros((half_rows, wide), F32)
        for t in range(taps):
            begin = HALO - (taps - 1) + t
            rows = slice(begin, begin + half_rows)
            gate = gate + gtaps[side, t : t + 1, part].astype(F32) * conv_g[rows, here]
            up = up + utaps[side, t : t + 1, part].astype(F32) * conv_u[rows, here]
        hid[:, here] = (gate / (1.0 + jnp.exp(-gate)) * up).astype(BF16)

    @pl.when(holds)
    def _():
        end_r[chip] = jnp.zeros(end_r.shape[1:], BF16)

    @pl.when(jnp.logical_not(holds))
    def _():
        kept[...] = jnp.zeros(kept.shape, F32)

    shared_wait(len(shared) - 1)

    def end_copy(i, c):
        there = core * chips + i
        return remote(
            end_s.at[c, i * rs : (i + 1) * rs, :],
            end_r.at[chip, c],
            fx_s.at[i],
            fx_r.at[chip, c // (chunks - 1)],
            (sp, there),
        )

    def end_in(k, i):
        at = slice(0, chunks - 1) if i == 0 else slice(chunks - 1, chunks)
        return remote(
            end_s.at[at, 0:rs, :], end_r.at[k, at], fx_s.at[0], fx_r.at[k, i], (sp, mate)
        )

    def end_out(i):
        held = end_s.at[:, i * rs : (i + 1) * rs, :]
        return remote(held, end_r.at[chip], fx_s.at[i], fx_r.at[chip, 0], (sp, mate))

    for c in range(chunks):
        here = slice(c * cols, (c + 1) * cols)
        product = jnp.dot(hid[...], dw[:, here], preferred_element_type=F32)
        end_s[c] = product.astype(BF16)
        for i in range(chips):

            @pl.when(core * chips + i != tp)
            def _(i=i, c=c):
                end_copy(i, c).start()

            @pl.when(core * chips + i == tp)
            def _(i=i, here=here, product=product):
                kept[:, here] = product[i * rs : (i + 1) * rs, :]

    @pl.when(holds)
    def _():
        kept[...] = kept[...] + res[pl.ds(held_row, rs), :]

    @pl.when(jnp.logical_not(holds))
    def _():
        res_copy().wait_recv()
        kept[...] = res_r[...].astype(F32)

    squares = jnp.zeros((rs, 1), F32)
    sums = []
    for c in range(chunks):
        here = slice(c * cols, (c + 1) * cols)
        if c in (0, chunks - 1):
            for k in range(chips):

                @pl.when(k * CORES + from_core != tp)
                def _(k=k, c=c):
                    end_in(k, c // (chunks - 1)).wait_recv()

        total = kept[:, here]
        for k in range(chips):
            total = total + end_r[k, c].astype(F32)
        squares = squares + jnp.sum(total * total, axis=-1, keepdims=True)
        sums.append(total)
    scale = lax.rsqrt(squares / width + EPS)
    for c in range(chunks):
        here = slice(c * cols, (c + 1) * cols)
        out_ref[:, here] = (sums[c] * scale * fgain[:, here]).astype(BF16)

    def sent(rows, sem):
        held = kv.at[0:rows, :]
        remote(held, held, sem, d2_r.at[0], (sp, mate)).wait_send()

    if chips > 1:
        sent((chips - 1) * r, kx_s)
    q_copy(core).wait_send()
    for i in range(len(shared)):
        pushed(i, core).wait_send()
    for k in range(1, chips):
        wide_all(k, slice(0, half_rows), chunks).wait_send()
    for i in range(chips):

        @pl.when(core * chips + i != tp)
        def _(i=i):
            end_out(i).wait_send()

    @pl.when(sends_halo)
    def _():
        halo.wait_send()

    @pl.when(sends_res)
    def _():
        res_copy().wait_send()

    sent(n * runs * run, d2_s)
    if n > 1:
        sent((full * CORES + (1 if last else 0)) * runs * run, ring_s)


def solution(mesh):
    n = mesh.shape["sp"]
    chips = mesh.shape["tp"] // CORES
    head = 256

    def shards(*args):
        args = [a[None, :] if a.ndim == 1 else a for a in args]
        (target, source, _, _, qw, kw, _, ow, _, gw, _, _, _, dw, _) = args
        tgt_rows, width = target.shape
        r = source.shape[0]
        kv_heads = kw.shape[1] // head
        heads_here = qw.shape[1] // head
        rs = tgt_rows // (CORES * chips)
        half = chips * rs
        cols = width // 4
        chunks = width // cols
        ff = gw.shape[1]
        wide = 256 if ff % 256 == 0 else 128
        q_rows = heads_here * tgt_rows
        sub = max(r // RUN, 1)
        runs = chips * sub
        dma = pltpu.SemaphoreType.DMA
        shapes = [a.shape for a in args]
        for i in (9, 10, 11, 12):
            shapes[i] = (CORES,) + shapes[i]
        for i in (7, 13):
            shapes[i] = (CORES * shapes[i][0], shapes[i][1])
        scratch = [pltpu.VMEM(shape, a.dtype) for shape, a in zip(shapes, args, strict=True)]
        scratch += [
            pltpu.VMEM((kv_heads, r, 2 * head), BF16),
            pltpu.VMEM((n * CORES * chips * r, 2 * head), BF16),
            pltpu.VMEM((q_rows, head), BF16),
            pltpu.VMEM((q_rows, 1), F32),
            pltpu.VMEM((q_rows, 1), F32),
            pltpu.VMEM((q_rows, head), F32),
            pltpu.VMEM((half, CORES * heads_here * head), BF16),
            pltpu.VMEM((chunks, half, cols), BF16),
            pltpu.VMEM((max(chips - 1, 1), chunks, half, cols), BF16),
            pltpu.VMEM((CORES, heads_here * half, head), BF16),
            pltpu.VMEM((half, width), F32),
            pltpu.VMEM((chunks, HALO + half, cols), BF16),
            pltpu.VMEM((chunks, HALO, cols), BF16),
            pltpu.VMEM((HALO + half, CORES * ff), F32),
            pltpu.VMEM((HALO + half, CORES * ff), F32),
            pltpu.VMEM((half, CORES * ff), BF16),
            pltpu.VMEM((chunks, half, cols), BF16),
            pltpu.VMEM((chips, chunks, rs, cols), BF16),
            pltpu.VMEM((rs, width), F32),
            pltpu.VMEM((rs, width), BF16),
            pltpu.VMEM((rs, width), BF16),
            dma((len(args) + 2 * kv_heads,)),
            dma,
            dma((max(runs - sub, 1),)),
            dma,
            dma((max(n // 2, 1), CORES, runs)),
            dma,
            dma((max(n // 2, 1),)),
            dma((runs,)),
        ]
        scratch += [dma] * 2
        scratch += [dma((6,))] * 2
        scratch += [dma((chips,)), dma((chips, chunks + 1))]
        scratch += [dma] * 4
        scratch += [dma((chips,)), dma((chips, 2))]
        return pl.pallas_call(
            functools.partial(layer, (n, chips, kv_heads, head, heads_here, cols, sub, wide)),
            out_shape=pltpu.VMEM((rs, width), BF16),
            in_specs=[pl.BlockSpec(memory_space=pl.ANY)] * len(args),
            out_specs=pl.BlockSpec(memory_space=pltpu.VMEM),
            scratch_shapes=scratch,
            compiler_params=pltpu.CompilerParams(
                collective_id=0, has_side_effects=True, vmem_limit_bytes=60 * 1024 * 1024
            ),
        )(*args)

    in_specs = (
        P("sp", None),
        P(("sp", "tp"), None),
        P(),
        P(),
        P(None, "tp"),
        P(),
        P(),
        P("tp", None),
        P(),
        P(None, "tp"),
        P(None, "tp"),
        P(None, "tp"),
        P(None, "tp"),
        P("tp", None),
        P(),
    )
    return jax.shard_map(
        shards, mesh=mesh, in_specs=in_specs, out_specs=P(("sp", "tp"), None), check_vma=False
    )
```

time: 44.3 us -> 39.7 us (0.90)
  Pallas kernels: 43.5 us -> 38.9 us
    pallas_call x1, Pallas kernels: 43.5 us -> 38.9 us  [shards(): pl.pallas_call(functools.partial(layer, (n, chips, kv_heads, head, heads_...]
where the time goes in v2:
time: 39.7 us; the launch traced here: 39.6 us
  Pallas kernels  38.9 us (98%)
  local copies, waits for them, and re-layouts  0.66 us (2%)
    pallas_call x1, Pallas kernels, shards(): pl.pallas_call(functools.partial(layer, (n, chips, kv_heads, head, heads_...  38.9 us

profile of v2, /device:TPU:0, one launch (start us, length us, event | category | flops | bytes accessed | tf_op | source)
XLA Modules:
  0.0 39.6 jit_solution(1241626766286496199)
XLA Ops:
  0.0 38.9 %shard_map.145 = bf16[32,2048]{1,0:T(8,128)(2,1)S(1)} custom-call(bf16[128,2048]{1,0:T(8,128)(2,1)} %target_h.1, bf16[64,2048]{1,0:T(8,128)(2,1)} %source_h.1, f32[1,2048]{1,0:T(1,128)} %bitcast.4, f32[1,2048]{1,0:T(1,128)} %bitcast.5, bf16[2048,512]{1,0:T(8,128)(2,1)} %qw_h.1, bf16[2048,512]{1,0:T(8,128)(2,1)} %kw_h.1, bf16[2048,512]{1,0:T(8,128)(2,1)} %vw_h.1, ...), custom_call_target="tpu_custom_call" | custom-call | tf_op jit(solution)/shard_map/pallas_call | solution.py:746
  38.9 0.7 %copy.17 = bf16[32,2048]{1,0:T(8,128)(2,1)} copy(bf16[32,2048]{1,0:T(8,128)(2,1)S(1)} %shard_map.145) | data formatting | bytes 262144

commit v3 on v2

--- a/solution.py
+++ b/solution.py
@@ -112,7 +112,8 @@
     chip = tp // CORES
     core = tp % CORES
     mate = tp + 1 - 2 * core
-    base = pl.multiple_of(core * half_rows, half_rows)
+    span = (core + chip) % CORES
+    base = pl.multiple_of(span * half_rows, half_rows)
 
     def chip_at(k):
         return (chip + k) % chips
@@ -157,7 +158,7 @@
     barrier = pltpu.get_barrier_semaphore()
     following = (sp + 1) % n
     peers = [(ahead, tp), (behind, tp), (sp, mate)]
-    peers += [(sp, chip_at(k) * CORES + core) for k in range(1, chips)]
+    peers += [(sp, chip_at(k) * CORES + i) for k in range(1, chips) for i in range(CORES)]
     for peer in peers:
         pl.semaphore_signal(barrier, inc=1, device_id=peer, device_id_type=MESH)
 
@@ -259,8 +260,14 @@
         pushed(i, 1 - core).wait_recv()
 
     def launch(j):
-        if n > 1:
+        if full >= 1 or (last and (0, j) in ends):
             ring_copy(1, 0, j).start()
+        elif last:
+
+            @pl.when(core == 1)
+            def _():
+                ring_copy(1, 0, j).start()
+
         mirror_out(0, 0, j).start()
 
     def launch_mate(blocks):
@@ -268,30 +275,51 @@
             mirror_in(0, 0, j).wait_recv()
             if full >= 1:
                 ring_copy(1, 1, j).start()
+            elif last and (1, j) in more:
+
+                @pl.when(core == 1)
+                def _(j=j):
+                    ring_copy(1, 1, j).start()
 
     def launch_far():
         for j in far:
             chip_copy(j).wait_recv()
             launch(j)
 
-    quota = {1: 5, 2: 4, 3: 3}
+    quota = {1: 6, 2: 5, 3: 1}
+    ends = [(0, j) for j in own]
+    more = [(rel, j) for rel in range(CORES) for j in far]
 
     def arrive(d, rel, blocks):
         end = isinstance(d, int) and d == full
         for j in blocks:
             ring_copy(d, rel, j).wait_recv()
-            if not end or (last and rel == 0):
+            if not end or (last and (rel, j) in ends):
                 ring_copy(d + 1, rel, j).start()
+            elif last and (rel, j) in more:
+
+                @pl.when(core == 1)
+                def _(rel=rel, j=j):
+                    ring_copy(last, rel, j).start()
+
             mirror_out(d, rel, j).start()
             if isinstance(d, int) and d in quota and quota[d] > 0:
                 quota[d] -= 1
                 feed(1)
 
-    def arrive_last(blocks):
+    def arrive_last():
         if last:
-            for j in blocks:
-                ring_copy(last, 0, j).wait_recv()
-                mirror_out(last, 0, j).start()
+            for rel, j in ends:
+                ring_copy(last, rel, j).wait_recv()
+                mirror_out(last, rel, j).start()
+
+            if more:
+
+                @pl.when(core == 1)
+                def _():
+                    for rel, j in more:
+                        ring_copy(last, rel, j).wait_recv()
+                        mirror_out(last, rel, j).start()
 
     for copy in first:
         copy.wait()
@@ -329,7 +357,7 @@
 
     def q_copy(side):
         return remote(
-            q_held.at[1 - core],
+            q_held.at[1 - span],
             q2.at[pl.ds(pl.multiple_of(side * group, group), group), :],
             q_s,
             q_r,
@@ -337,7 +365,7 @@
         )
 
     q_copy(core).start()
-    q2[pl.ds(pl.multiple_of(core * group, group), group), :] = q_held[core]
+    q2[pl.ds(pl.multiple_of(core * group, group), group), :] = q_held[span]
     top[...] = jnp.full(top.shape, -1e30, F32)
     tot[...] = jnp.zeros(tot.shape, F32)
     acc[...] = jnp.zeros(acc.shape, F32)
@@ -367,14 +395,26 @@
         pairs += [(mgain_h, mgain), (fgain_h, fgain)]
         return [load(used + 3 + i, a, b) for i, (a, b) in enumerate(pairs)]
 
+    def mirror_wait(d, start, rows):
+        held = kv.at[pl.ds(start, rows), :]
+        remote(held, held, d2_s, d2_r.at[d - 1], (sp, mate)).wait_recv()
+
     def mirrored(d):
-        end = isinstance(d, int) and d == last
-        rows = slot_rows // CORES if end else slot_rows
-        start = slot_of(d, 1 - core) * slot_rows
-        if end:
-            start = start + (1 - core) * rows
-        held = kv.at[pl.ds(pl.multiple_of(start, rows), rows), :]
-        remote(held, held, d2_s, d2_r.at[d - 1], (sp, mate)).wait_recv()
+        if isinstance(d, int) and d == last:
+            begin = (n - 1) * slot_rows
+
+            @pl.when(core == 1)
+            def _():
+                mirror_wait(d, begin, len(ends) * run)
+
+            if more:
+
+                @pl.when(core == 0)
+                def _():
+                    mirror_wait(d, begin + len(ends) * run, slot_rows - len(ends) * run)
+        else:
+            start = slot_of(d, 1 - core) * slot_rows
+            mirror_wait(d, pl.multiple_of(start, slot_rows), slot_rows)
 
     def wave(d):
         for blocks in (own, far):
@@ -382,7 +422,7 @@
                 arrive(d, rel, blocks)
 
     if full >= 1:
-        feed(2)
+        feed(4)
         launch_mate(own)
         launch_far()
         feed(3)
@@ -411,8 +451,8 @@
         for d in range(done, full):
             mirrored(d)
         attend(start, 2 * full - 1 - start)
-        arrive_last(range(runs))
-        feed(len(pending) - SPLIT)
+        arrive_last()
+        feed(len(pending) - SPLIT // 2)
         mirrored(full)
         attend(2 * full - 1, 2)
     else:
@@ -420,7 +460,7 @@
         launch_far()
         launch_mate(range(runs))
         q_copy(1 - core).wait_recv()
-        arrive_last(range(runs))
+        arrive_last()
         feed(3 * SPLIT + 2)
         attend(0, 1)
     if last:
@@ -437,6 +477,10 @@
     body_rows = half_rows - HALO
     body = slice(0, body_rows)
     tail = slice(body_rows, half_rows)
+
+    def peer_of(k):
+        there = chip_at(k)
+        return there * CORES + (span + there) % CORES
 
     def wide_copy(k, c, i):
         at = (body, tail)[i]
@@ -445,7 +489,7 @@
             chip_r.at[k - 1, c, at, :],
             bx_s.at[k],
             bx_r.at[k, c * (1 - i) + chunks * i],
-            (sp, chip_at(k) * CORES + core),
+            (sp, peer_of(k)),
         )
 
     for c in range(chunks):
@@ -465,7 +509,7 @@
             chip_r.at[k - 1, :, at, :],
             bx_s.at[k],
             bx_r.at[k, recv],
-            (sp, chip_at(k) * CORES + core),
+            (sp, peer_of(k)),
         )
 
     def settle(c, i):
@@ -483,12 +527,12 @@
     for k in range(1, chips):
         wide_all(k, tail, chunks).wait_recv()
 
-    beyond = sp * (1 - core) + following * core
+    beyond = sp * (1 - span) + following * span
 
     halo = remote(halo_s, rows_in.at[:, 0:HALO, :], h_s, h_r, (beyond, mate))
 
-    sends_halo = jnp.logical_or(core == 0, sp < n - 1)
-    takes_halo = jnp.logical_or(core == 1, sp > 0)
+    sends_halo = jnp.logical_or(span == 0, sp < n - 1)
+    takes_halo = jnp.logical_or(span == 1, sp > 0)
     tail_squares = settle(0, 1)
     for c in range(1, chunks):
         tail_squares = tail_squares + settle(c, 1)
@@ -531,20 +575,22 @@
         squares = squares + settle(c, 0)
         here = slice(c * cols, (c + 1) * cols)
         rows_in[c, HALO:, :] = (res[:, here] * mgain[:, here]).astype(BF16)
-        if c == chunks - 2:
+        if c == 1:
             ready()
-            for i in range(chunks - 1):
+            mix(0)
+        elif c == chunks - 2:
+            for i in range(1, chunks - 1):
                 mix(i)
     squares = jnp.concatenate([squares, tail_squares], axis=0)
     scale = jnp.concatenate(
         [jnp.ones((HALO, 1), F32), lax.rsqrt(squares / width + EPS)], axis=0
     )
 
-    from_core = tp // chips
+    source = tp // chips
     held_row = pl.multiple_of((tp % chips) * rs, rs)
     mate_row = pl.multiple_of((mate % chips) * rs, rs)
-    sends_res = mate // chips == core
-    holds = from_core == core
+    sends_res = mate // chips == span
+    holds = source == span
 
     def res_copy():
         return remote(res_s, res_r, r_s, r_r, (sp, mate))
@@ -586,7 +632,7 @@
     shared_wait(len(shared) - 1)
 
     def end_copy(i, c):
-        there = core * chips + i
+        there = span * chips + i
         return remote(
             end_s.at[c, i * rs : (i + 1) * rs, :],
             end_r.at[chip, c],
@@ -611,11 +657,11 @@
         end_s[c] = product.astype(BF16)
         for i in range(chips):
 
-            @pl.when(core * chips + i != tp)
+            @pl.when(span * chips + i != tp)
             def _(i=i, c=c):
                 end_copy(i, c).start()
 
-            @pl.when(core * chips + i == tp)
+            @pl.when(span * chips + i == tp)
             def _(i=i, here=here, product=product):
                 kept[:, here] = product[i * rs : (i + 1) * rs, :]
 
@@ -635,7 +681,7 @@
         if c in (0, chunks - 1):
             for k in range(chips):
 
-                @pl.when(k * CORES + from_core != tp)
+                @pl.when(k * CORES + (source + k) % CORES != tp)
                 def _(k=k, c=c):
                     end_in(k, c // (chunks - 1)).wait_recv()
 
@@ -662,7 +708,7 @@
         wide_all(k, slice(0, half_rows), chunks).wait_send()
     for i in range(chips):
 
-        @pl.when(core * chips + i != tp)
+        @pl.when(span * chips + i != tp)
         def _(i=i):
             end_out(i).wait_send()
 
@@ -674,9 +720,16 @@
     def _():
         res_copy().wait_send()
 
-    sent(n * runs * run, d2_s)
-    if n > 1:
-        sent((full * CORES + (1 if last else 0)) * runs * run, ring_s)
+    ring_rows = full * CORES * runs * run
+    mirror_rows = ring_rows + runs * run
+    for side in range(CORES if last else 1):
+        extra = (len(ends) + side * len(more)) * run if last else 0
+
+        @pl.when(jnp.logical_or(core == side, not last))
+        def _(extra=extra):
+            sent(mirror_rows + extra, d2_s)
+            if ring_rows + extra:
+                sent(ring_rows + extra, ring_s)
 
 
 def solution(mesh):

time: 39.7 us -> 37.3 us (0.940)
  Pallas kernels: 38.9 us -> 36.5 us
    pallas_call x1, Pallas kernels: 38.9 us -> 36.5 us  [shards(): pl.pallas_call(functools.partial(layer, (n, chips, kv_heads, head, heads_...]
where the time goes in v3:
time: 37.3 us; the launch traced here: 37.2 us
  Pallas kernels  36.5 us (98%)
  local copies, waits for them, and re-layouts  0.66 us (2%)
    pallas_call x1, Pallas kernels, shards(): pl.pallas_call(functools.partial(layer, (n, chips, kv_heads, head, heads_...  36.5 us

profile of v3, /device:TPU:0, one launch (start us, length us, event | category | flops | bytes accessed | tf_op | source)
XLA Modules:
  0.0 37.2 jit_solution(11982893473115658913)
XLA Ops:
  0.0 36.5 %shard_map.145 = bf16[32,2048]{1,0:T(8,128)(2,1)S(1)} custom-call(bf16[128,2048]{1,0:T(8,128)(2,1)} %target_h.1, bf16[64,2048]{1,0:T(8,128)(2,1)} %source_h.1, f32[1,2048]{1,0:T(1,128)} %bitcast.4, f32[1,2048]{1,0:T(1,128)} %bitcast.5, bf16[2048,512]{1,0:T(8,128)(2,1)} %qw_h.1, bf16[2048,512]{1,0:T(8,128)(2,1)} %kw_h.1, bf16[2048,512]{1,0:T(8,128)(2,1)} %vw_h.1, ...), custom_call_target="tpu_custom_call" | custom-call | tf_op jit(solution)/shard_map/pallas_call | solution.py:799
  36.5 0.7 %copy.17 = bf16[32,2048]{1,0:T(8,128)(2,1)} copy(bf16[32,2048]{1,0:T(8,128)(2,1)S(1)} %shard_map.145) | data formatting | bytes 262144

commit v4 on v3

--- a/solution.py
+++ b/solution.py
@@ -178,13 +178,14 @@
             start = pl.multiple_of(start, run)
         return kv.at[pl.ds(start, run), :]
 
-    def chip_copy(j):
+    def chip_copy(j, half):
         there = chip_at(j // sub)
+        at = slice(half * head, (half + 1) * head)
         return remote(
-            kvh.at[head_of(there), (j % sub) * run : (j % sub + 1) * run, :],
-            block(0, core, j),
+            kvh.at[head_of(there), (j % sub) * run : (j % sub + 1) * run, at],
+            block(0, core, j).at[:, at],
             kx_s,
-            kx_r.at[j - sub],
+            kx_r.at[j - sub, half],
             (sp, there * CORES + core),
         )
 
@@ -283,7 +284,8 @@
 
     def launch_far():
         for j in far:
-            chip_copy(j).wait_recv()
+            chip_copy(j, 0).wait_recv()
+            chip_copy(j, 1).wait_recv()
             launch(j)
 
     quota = {1: 6, 2: 5, 3: 1}
@@ -329,17 +331,23 @@
         for i, (a, b) in enumerate(((target_h, tgt), (qgain_h, qgain), (qw_h, qw)))
     ]
     early = chips == kv_heads
+
+    def send_far(half):
+        for j in far:
+            chip_copy(j, half).start()
+
     for i, g in enumerate(order):
-        for copy in by_head[i]:
-            copy.wait()
-        keys = jnp.dot(source_in, kw[:, columns(g)], preferred_element_type=F32)
-        kvh[g, :, :head] = keys.astype(BF16)
-        values = jnp.dot(source_in, vw[:, columns(g)], preferred_element_type=F32)
-        kvh[g, :, head:] = values.astype(BF16)
-        if i == (kv_heads - 2 if early else kv_heads - 1):
-            pl.semaphore_wait(barrier, len(peers))
-            for j in range(sub, runs):
-                chip_copy(j).start()
+        for half, copy in enumerate(by_head[i]):
+            if i == 0 or half == 0:
+                for waited in by_head[i] if i else [copy]:
+                    waited.wait()
+            weight = (kw, vw)[half]
+            product = jnp.dot(source_in, weight[:, columns(g)], preferred_element_type=F32)
+            kvh[g, :, half * head : (half + 1) * head] = product.astype(BF16)
+            if i == (kv_heads - 2 if early else kv_heads - 1):
+                if half == 0:
+                    pl.semaphore_wait(barrier, len(peers))
+                send_far(half)
     kv[pl.ds(pl.multiple_of(core * chips * r, r), r), :] = kvh[own_head]
     for j in range(sub):
         launch(j)
@@ -529,7 +537,12 @@
 
     beyond = sp * (1 - span) + following * span
 
-    halo = remote(halo_s, rows_in.at[:, 0:HALO, :], h_s, h_r, (beyond, mate))
+    halo = remote(halo_s, rows_in.at[:, 0:HALO, :], h_s, h_r.at[0], (beyond, mate))
+
+    def halo_copy(c):
+        return remote(
+            halo_s.at[c], rows_in.at[c, 0:HALO, :], h_s, h_r.at[c], (beyond, mate)
+        )
 
     sends_halo = jnp.logical_or(span == 0, sp < n - 1)
     takes_halo = jnp.logical_or(span == 1, sp > 0)
@@ -543,7 +556,8 @@
 
     @pl.when(sends_halo)
     def _():
-        halo.start()
+        for c in range(chunks):
+            halo_copy(c).start()
 
     feed(len(pending))
 
@@ -551,10 +565,10 @@
     def _():
         rows_in[:, 0:HALO, :] = jnp.zeros((chunks, HALO, cols), BF16)
 
-    def ready():
+    def ready(c):
         @pl.when(takes_halo)
         def _():
-            halo.wait_recv()
+            halo_copy(c).wait_recv()
 
     def mix(c):
         here = slice(c * cols, (c + 1) * cols)
@@ -575,12 +589,11 @@
         squares = squares + settle(c, 0)
         here = slice(c * cols, (c + 1) * cols)
         rows_in[c, HALO:, :] = (res[:, here] * mgain[:, here]).astype(BF16)
-        if c == 1:
-            ready()
-            mix(0)
-        elif c == chunks - 2:
-            for i in range(1, chunks - 1):
+        if 0 < c < chunks - 1:
+            for i in range(0 if c == 1 else c, c + 1):
+                ready(i)
                 mix(i)
+    ready(chunks - 1)
     squares = jnp.concatenate([squares, tail_squares], axis=0)
     scale = jnp.concatenate(
         [jnp.ones((HALO, 1), F32), lax.rsqrt(squares / width + EPS)], axis=0
@@ -784,7 +797,7 @@
             pltpu.VMEM((rs, width), BF16),
             dma((len(args) + 2 * kv_heads,)),
             dma,
-            dma((max(runs - sub, 1),)),
+            dma((max(runs - sub, 1), 2)),
             dma,
             dma((max(n // 2, 1), CORES, runs)),
             dma,
@@ -794,7 +807,7 @@
         scratch += [dma] * 2
         scratch += [dma((6,))] * 2
         scratch += [dma((chips,)), dma((chips, chunks + 1))]
-        scratch += [dma] * 4
+        scratch += [dma, dma((chunks,)), dma, dma]
         scratch += [dma((chips,)), dma((chips, 2))]
         return pl.pallas_call(
             functools.partial(layer, (n, chips, kv_heads, head, heads_here, cols, sub, wide)),

time: 37.3 us -> 37.1 us (level)
  no operation moved by 1% of the time
where the time goes in v4:
time: 37.1 us; the launch traced here: 36.9 us
  Pallas kernels  36.3 us (98%)
  local copies, waits for them, and re-layouts  0.66 us (2%)
    pallas_call x1, Pallas kernels, shards(): pl.pallas_call(functools.partial(layer, (n, chips, kv_heads, head, heads_...  36.3 us

profile of v4, /device:TPU:0, one launch (start us, length us, event | category | flops | bytes accessed | tf_op | source)
XLA Modules:
  0.0 36.9 jit_solution(16458357008407688913)
XLA Ops:
  0.0 36.3 %shard_map.145 = bf16[32,2048]{1,0:T(8,128)(2,1)S(1)} custom-call(bf16[128,2048]{1,0:T(8,128)(2,1)} %target_h.1, bf16[64,2048]{1,0:T(8,128)(2,1)} %source_h.1, f32[1,2048]{1,0:T(1,128)} %bitcast.4, f32[1,2048]{1,0:T(1,128)} %bitcast.5, bf16[2048,512]{1,0:T(8,128)(2,1)} %qw_h.1, bf16[2048,512]{1,0:T(8,128)(2,1)} %kw_h.1, bf16[2048,512]{1,0:T(8,128)(2,1)} %vw_h.1, ...), custom_call_target="tpu_custom_call" | custom-call | tf_op jit(solution)/shard_map/pallas_call | solution.py:812
  36.3 0.7 %copy.17 = bf16[32,2048]{1,0:T(8,128)(2,1)} copy(bf16[32,2048]{1,0:T(8,128)(2,1)S(1)} %shard_map.145) | data formatting | bytes 262144

commit v5 on v4

--- a/solution.py
+++ b/solution.py
@@ -495,8 +495,8 @@
         return remote(
             chip_s.at[c, at, :],
             chip_r.at[k - 1, c, at, :],
-            bx_s.at[k],
-            bx_r.at[k, c * (1 - i) + chunks * i],
+            bx_s.at[k - 1],
+            bx_r.at[k - 1, c * (1 - i) + chunks * i],
             (sp, peer_of(k)),
         )
 
@@ -515,8 +515,8 @@
         return remote(
             chip_s.at[:, at, :],
             chip_r.at[k - 1, :, at, :],
-            bx_s.at[k],
-            bx_r.at[k, recv],
+            bx_s.at[k - 1],
+            bx_r.at[k - 1, recv],
             (sp, peer_of(k)),
         )
 
@@ -537,12 +537,7 @@
 
     beyond = sp * (1 - span) + following * span
 
-    halo = remote(halo_s, rows_in.at[:, 0:HALO, :], h_s, h_r.at[0], (beyond, mate))
-
-    def halo_copy(c):
-        return remote(
-            halo_s.at[c], rows_in.at[c, 0:HALO, :], h_s, h_r.at[c], (beyond, mate)
-        )
+    halo = remote(halo_s, rows_in.at[:, 0:HALO, :], h_s, h_r, (beyond, mate))
 
     sends_halo = jnp.logical_or(span == 0, sp < n - 1)
     takes_halo = jnp.logical_or(span == 1, sp > 0)
@@ -556,8 +551,7 @@
 
     @pl.when(sends_halo)
     def _():
-        for c in range(chunks):
-            halo_copy(c).start()
+        halo.start()
 
     feed(len(pending))
 
@@ -565,10 +559,10 @@
     def _():
         rows_in[:, 0:HALO, :] = jnp.zeros((chunks, HALO, cols), BF16)
 
-    def ready(c):
+    def ready():
         @pl.when(takes_halo)
         def _():
-            halo_copy(c).wait_recv()
+            halo.wait_recv()
 
     def mix(c):
         here = slice(c * cols, (c + 1) * cols)
@@ -589,11 +583,11 @@
         squares = squares + settle(c, 0)
         here = slice(c * cols, (c + 1) * cols)
         rows_in[c, HALO:, :] = (res[:, here] * mgain[:, here]).astype(BF16)
+        if c == 1:
+            ready()
         if 0 < c < chunks - 1:
             for i in range(0 if c == 1 else c, c + 1):
-                ready(i)
                 mix(i)
-    ready(chunks - 1)
     squares = jnp.concatenate([squares, tail_squares], axis=0)
     scale = jnp.concatenate(
         [jnp.ones((HALO, 1), F32), lax.rsqrt(squares / width + EPS)], axis=0
@@ -644,11 +638,11 @@
 
     shared_wait(len(shared) - 1)
 
-    def end_copy(i, c):
+    def end_copy(i, c, at):
         there = span * chips + i
         return remote(
-            end_s.at[c, i * rs : (i + 1) * rs, :],
-            end_r.at[chip, c],
+            end_s.at[c, i * rs : (i + 1) * rs, at],
+            end_r.at[chip, c].at[:, at],
             fx_s.at[i],
             fx_r.at[chip, c // (chunks - 1)],
             (sp, there),
@@ -664,15 +658,18 @@
         held = end_s.at[:, i * rs : (i + 1) * rs, :]
         return remote(held, end_r.at[chip], fx_s.at[i], fx_r.at[chip, 0], (sp, mate))
 
-    for c in range(chunks):
-        here = slice(c * cols, (c + 1) * cols)
+    parts = [(0, 0, cols // 2), (0, cols // 2, cols)]
+    parts += [(c, 0, cols) for c in range(1, chunks)]
+    for c, low, high in parts:
+        at = slice(low, high)
+        here = slice(c * cols + low, c * cols + high)
         product = jnp.dot(hid[...], dw[:, here], preferred_element_type=F32)
-        end_s[c] = product.astype(BF16)
+        end_s[c, :, at] = product.astype(BF16)
         for i in range(chips):
 
             @pl.when(span * chips + i != tp)
-            def _(i=i, c=c):
-                end_copy(i, c).start()
+            def _(i=i, c=c, at=at):
+                end_copy(i, c, at).start()
 
             @pl.when(span * chips + i == tp)
             def _(i=i, here=here, product=product):
@@ -795,7 +792,7 @@
             pltpu.VMEM((rs, width), F32),
             pltpu.VMEM((rs, width), BF16),
             pltpu.VMEM((rs, width), BF16),
-            dma((len(args) + 2 * kv_heads,)),
+            dma((len(args) - 2 + 2 * kv_heads,)),
             dma,
             dma((max(runs - sub, 1), 2)),
             dma,
@@ -806,8 +803,8 @@
         ]
         scratch += [dma] * 2
         scratch += [dma((6,))] * 2
-        scratch += [dma((chips,)), dma((chips, chunks + 1))]
-        scratch += [dma, dma((chunks,)), dma, dma]
+        scratch += [dma((max(chips - 1, 1),)), dma((max(chips - 1, 1), chunks + 1))]
+        scratch += [dma] * 4
         scratch += [dma((chips,)), dma((chips, 2))]
         return pl.pallas_call(
             functools.partial(layer, (n, chips, kv_heads, head, heads_here, cols, sub, wide)),

time: 37.1 us -> 36.9 us (level)
  no operation moved by 1% of the time
where the time goes in v5:
time: 36.9 us; the launch traced here: 36.7 us
  Pallas kernels  36.1 us (98%)
  local copies, waits for them, and re-layouts  0.66 us (2%)
    pallas_call x1, Pallas kernels, shards(): pl.pallas_call(functools.partial(layer, (n, chips, kv_heads, head, heads_...  36.1 us

profile of v5, /device:TPU:0, one launch (start us, length us, event | category | flops | bytes accessed | tf_op | source)
XLA Modules:
  0.0 36.7 jit_solution(8775659831790672582)
XLA Ops:
  0.0 36.1 %shard_map.145 = bf16[32,2048]{1,0:T(8,128)(2,1)S(1)} custom-call(bf16[128,2048]{1,0:T(8,128)(2,1)} %target_h.1, bf16[64,2048]{1,0:T(8,128)(2,1)} %source_h.1, f32[1,2048]{1,0:T(1,128)} %bitcast.4, f32[1,2048]{1,0:T(1,128)} %bitcast.5, bf16[2048,512]{1,0:T(8,128)(2,1)} %qw_h.1, bf16[2048,512]{1,0:T(8,128)(2,1)} %kw_h.1, bf16[2048,512]{1,0:T(8,128)(2,1)} %vw_h.1, ...), custom_call_target="tpu_custom_call" | custom-call | tf_op jit(solution)/shard_map/pallas_call | solution.py:809
  36.1 0.7 %copy.17 = bf16[32,2048]{1,0:T(8,128)(2,1)} copy(bf16[32,2048]{1,0:T(8,128)(2,1)S(1)} %shard_map.145) | data formatting | bytes 262144

commit v6 on v5

--- a/solution.py
+++ b/solution.py
@@ -434,9 +434,21 @@
         launch_mate(own)
         launch_far()
         feed(3)
-        launch_mate(far)
+
+        @pl.when(core == 0)
+        def _():
+            launch_mate(far)
+
+        arrive(1, 0, own)
+
+        @pl.when(core == 1)
+        def _():
+            launch_mate(far)
+
         q_copy(1 - core).wait_recv()
-        wave(1)
+        arrive(1, 1, own)
+        arrive(1, 0, far)
+        arrive(1, 1, far)
         rest = local_loads()
         done = 1
         if full > 4:

time: 36.9 us -> 36.9 us (level)
  no operation moved by 1% of the time
where the time goes in v6:
time: 36.9 us; the launch traced here: 36.7 us
  Pallas kernels  36.1 us (98%)
  local copies, waits for them, and re-layouts  0.66 us (2%)
    pallas_call x1, Pallas kernels, shards(): pl.pallas_call(functools.partial(layer, (n, chips, kv_heads, head, heads_...  36.1 us

profile of v6, /device:TPU:0, one launch (start us, length us, event | category | flops | bytes accessed | tf_op | source)
XLA Modules:
  0.0 36.7 jit_solution(18040152295707335229)
XLA Ops:
  0.0 36.1 %shard_map.145 = bf16[32,2048]{1,0:T(8,128)(2,1)S(1)} custom-call(bf16[128,2048]{1,0:T(8,128)(2,1)} %target_h.1, bf16[64,2048]{1,0:T(8,128)(2,1)} %source_h.1, f32[1,2048]{1,0:T(1,128)} %bitcast.4, f32[1,2048]{1,0:T(1,128)} %bitcast.5, bf16[2048,512]{1,0:T(8,128)(2,1)} %qw_h.1, bf16[2048,512]{1,0:T(8,128)(2,1)} %kw_h.1, bf16[2048,512]{1,0:T(8,128)(2,1)} %vw_h.1, ...), custom_call_target="tpu_custom_call" | custom-call | tf_op jit(solution)/shard_map/pallas_call | solution.py:821
  36.1 0.7 %copy.17 = bf16[32,2048]{1,0:T(8,128)(2,1)} copy(bf16[32,2048]{1,0:T(8,128)(2,1)S(1)} %shard_map.145) | data formatting | bytes 262144
